TPU v7x, 32 devices: a whole 2x2x4 slice. The times are simulated.
32 devices in a mesh: ep: 16 (over z, y, x), tp: 2 (over core).
Axes of the slice: x: 2, y: 2, z: 4, core: 2. Of those that a mesh axis runs over, the one named last changes fastest.
Arguments:
- hidden: bfloat16 [256, 2048], P('ep'), may hold values from -6 to 6
- attn_gain: bfloat16 [2048], replicated, may hold values from 0.099609375 to 1.8984375
- query_weight: bfloat16 [2048, 2048], P(None, 'tp'), may hold values from -0.125 to 0.125
- key_weight: bfloat16 [2048, 128], P(None, 'tp'), may hold values from -0.125 to 0.125
- value_weight: bfloat16 [2048, 128], P(None, 'tp'), may hold values from -0.125 to 0.125
- forget_weight: bfloat16 [2048, 32], P(None, 'tp'), may hold values from -0.125 to 0.125
- forget_bias: float32 [32], P('tp'), may hold values from -1 to 4
- cache_keys: bfloat16 [256, 2, 64, 1024], P('ep', 'tp'), may hold values from -64 to 64
- cache_values: bfloat16 [256, 2, 64, 1024], P('ep', 'tp'), may hold values from -6 to 6
- cache_logsum: float32 [256, 32, 1024], P('ep', 'tp'), may hold values from -144 to 0, as said below
- lengths: int32 [256], P('ep'), may hold values from 2 to 1023, as said below
- out_weight: bfloat16 [2048, 2048], P('ep'), may hold values from -0.125 to 0.125
- ffn_gain: bfloat16 [2048], replicated, may hold values from 0.099609375 to 1.8984375
- expert_ids: int32 [256, 6], P('ep'), may hold values from 0 to 15, all different within a row; in each aligned block of 16 rows (0 to 15, 16 to 31, ...) at most 12 rows name the same one
- expert_scores: float32 [256, 6], P('ep'), may hold values from 0.1 to 1
- gate_weights: bfloat16 [16, 2048, 512], P('ep', None, 'tp'), may hold values from -0.125 to 0.125
- up_weights: bfloat16 [16, 2048, 512], P('ep', None, 'tp'), may hold values from -0.125 to 0.125
- down_weights: bfloat16 [16, 512, 2048], P('ep', 'tp'), may hold values from -0.25 to 0.25
Outputs:
- updated: bfloat16 [256, 2048], P('ep')
- new_key: bfloat16 [256, 2, 64], P('ep', 'tp')
- new_value: bfloat16 [256, 2, 64], P('ep', 'tp')
- new_logsum: float32 [256, 32], P('ep', 'tp')
Inputs may be any that keep to these rules, and one draw needn't show every extreme that they name: `cache_logsum`: non-increasing along the positions. The new token stands at position lengths; some sequence has 1023 cached positions. `expert_ids`: each row names 6 different experts; the rows of one index of ep name one expert at most 12 times.
All inputs are finite; a program needn't handle non-finite values.
Results may differ from a plain program's by a relative error of at most 0.006.
Values may be sent and summed in bfloat16 or wider, within the bound.
A program may use at most 64 MiB of HBM per device.

v0:
```python
import functools
import math

import jax
import jax.numpy as jnp
from jax import lax
from jax.experimental import pallas as pl
from jax.experimental.pallas import tpu as pltpu
from jax.sharding import PartitionSpec as P

HD = 64
TOP_K = 6


epsilon = 1e-06


def root_norm(values_in, gain):
    floats = values_in.astype(jnp.float32)
    inv_root = lax.rsqrt(jnp.mean(floats * floats, axis=-1, keepdims=True) + epsilon)
    return floats * inv_root * gain.astype(jnp.float32)


def attend(hidden, attn_gain, query_weight, key_weight, value_weight, forget_weight, forget_bias,
           cache_keys, cache_values, cache_logsum, lengths):
    rows_here = hidden.shape[0]
    query_heads = query_weight.shape[1] // HD
    key_heads = key_weight.shape[1] // HD
    group_size = query_heads // key_heads
    cache_len = cache_keys.shape[-1]
    score_scale = HD ** (-0.5)
    normed = root_norm(hidden, attn_gain).astype(jnp.bfloat16)
    queries = jnp.dot(normed, query_weight, preferred_element_type=jnp.float32).astype(jnp.bfloat16)
    key_new = (
        jnp.dot(normed, key_weight, preferred_element_type=jnp.float32)
        .astype(jnp.bfloat16)
        .reshape(rows_here, key_heads, HD)
    )
    value_new = (
        jnp.dot(normed, value_weight, preferred_element_type=jnp.float32)
        .astype(jnp.bfloat16)
        .reshape(rows_here, key_heads, HD)
    )
    log_forget = jax.nn.log_sigmoid(
        jnp.dot(normed, forget_weight, preferred_element_type=jnp.float32) + forget_bias
    )
    positions = jnp.arange(cache_len, dtype=jnp.int32)
    is_last = positions[None, :] == (lengths - 1)[:, None]
    new_logsum = jnp.sum(jnp.where(is_last[:, None, :], cache_logsum, 0.0), axis=-1) + log_forget
    grouped = queries.reshape(rows_here, key_heads, group_size, HD)
    scores = jnp.einsum("sgjd,sgdp->sgjp", grouped, cache_keys, preferred_element_type=jnp.float32)
    scores = scores.reshape(rows_here, query_heads, cache_len) * score_scale
    scores = scores + new_logsum[:, :, None] - cache_logsum
    is_live = positions[None, :] < lengths[:, None]
    scores = jnp.where(is_live[:, None, :], scores, -jnp.inf)
    own_score = (
        jnp.einsum("sgjd,sgd->sgj", grouped, key_new, preferred_element_type=jnp.float32).reshape(
            rows_here, query_heads
        )
        * score_scale
    )
    top_score = jnp.maximum(jnp.max(scores, axis=-1), own_score)
    past_exp = jnp.exp(scores - top_score[:, :, None])
    own_exp = jnp.exp(own_score - top_score)
    denominator = jnp.sum(past_exp, axis=-1) + own_exp
    past_weight = (past_exp / denominator[:, :, None]).astype(jnp.bfloat16)
    own_weight = (own_exp / denominator).astype(jnp.bfloat16)
    attended = jnp.einsum(
        "sgjp,sgdp->sgjd",
        past_weight.reshape(rows_here, key_heads, group_size, cache_len),
        cache_values,
        preferred_element_type=jnp.float32,
    )
    attended = (
        attended
        + own_weight.astype(jnp.float32).reshape(rows_here, key_heads, group_size)[:, :, :, None]
        * value_new.astype(jnp.float32)[:, :, None, :]
    )
    attended = attended.reshape(rows_here, query_heads * HD).astype(jnp.bfloat16)
    return attended, key_new, value_new, new_logsum


def rest_general(attended, hidden, out_weight, ffn_gain, expert_ids, expert_scores,
                 gate_weights, up_weights, down_weights):
    rows_here = hidden.shape[0]
    whole_heads = lax.all_gather(attended, "tp", axis=1, tiled=True)
    projected = lax.dot_general(
        lax.all_gather(whole_heads, "ep", axis=0, tiled=True),
        out_weight,
        (((1,), (1,)), ((), ())),
        preferred_element_type=jnp.float32,
    ).astype(jnp.bfloat16)
    mixed = lax.all_to_all(projected, "ep", split_axis=0, concat_axis=1, tiled=True)
    residual = hidden.astype(jnp.float32) + mixed.astype(jnp.float32)
    ffn_in = root_norm(residual, ffn_gain).astype(jnp.bfloat16)
    ep_size = lax.axis_size("ep")
    local_experts = gate_weights.shape[0]
    experts = ep_size * local_experts
    route_count = rows_here * TOP_K
    capacity = 2 * ((route_count + experts - 1) // experts)
    flat_ids = expert_ids.reshape(route_count)
    onehot = (flat_ids[:, None] == jnp.arange(experts, dtype=jnp.int32)[None, :]).astype(jnp.int32)
    running = jnp.cumsum(onehot, axis=0)
    slot_index = jnp.sum(running * onehot, axis=1) - 1
    target = flat_ids * capacity + slot_index
    dispatch_map = (
        target[:, None] == jnp.arange(experts * capacity, dtype=jnp.int32)[None, :]
    ).astype(jnp.bfloat16)
    route_rows = jnp.repeat(ffn_in, TOP_K, axis=0)
    outgoing = lax.dot_general(
        dispatch_map, route_rows, (((0,), (0,)), ((), ())), preferred_element_type=jnp.float32
    )
    outgoing = outgoing.astype(jnp.bfloat16).reshape(
        ep_size, local_experts, capacity, ffn_in.shape[1]
    )
    arrived = lax.all_to_all(outgoing, "ep", split_axis=0, concat_axis=0, tiled=True)
    gate_act = jnp.einsum(
        "sekd,edf->sekf", arrived, gate_weights, preferred_element_type=jnp.float32
    )
    up_act = jnp.einsum("sekd,edf->sekf", arrived, up_weights, preferred_element_type=jnp.float32)
    hidden_act = (jax.nn.silu(gate_act) * up_act).astype(jnp.bfloat16)
    partial_out = jnp.einsum(
        "sekf,efd->sekd", hidden_act, down_weights, preferred_element_type=jnp.float32
    )
    half_sum = lax.psum_scatter(
        partial_out.astype(jnp.bfloat16), "tp", scatter_dimension=3, tiled=True
    )
    sent_back = lax.all_to_all(half_sum, "ep", split_axis=0, concat_axis=0, tiled=True)
    share_width = sent_back.shape[-1]
    picked = jnp.dot(
        dispatch_map,
        sent_back.reshape(experts * capacity, share_width),
        preferred_element_type=jnp.float32,
    )
    route_weight = expert_scores / jnp.sum(expert_scores, axis=-1, keepdims=True)
    expert_mix = jnp.sum(
        picked.reshape(rows_here, TOP_K, share_width) * route_weight[:, :, None], axis=1
    )
    own_part = lax.dynamic_slice_in_dim(
        residual, lax.axis_index("tp") * share_width, share_width, 1
    )
    updated = lax.all_gather((own_part + expert_mix).astype(jnp.bfloat16), "tp", axis=1, tiled=True)
    return updated


MESH = pl.DeviceIdType.MESH


def rest_body(n, att_ref, hid_ref, gain_ref, mix_ref, ow_hbm, gate_hbm, up_hbm, down_hbm, out_ref,
              heads, ow, gate, up, down, part, part_in, proj, mixed, resid, rows, act, eout, back, sums, mix, upd,
              send, recv, pair_send, pair_recv, local):
    me, tp = lax.axis_index("ep"), lax.axis_index("tp")
    seqs, width = hid_ref.shape
    half = width // 2
    feats = ow.shape[0]
    cols = att_ref.shape[1]
    inner = math.isqrt(n)
    outer = n // inner
    line, spot = me // inner, lax.rem(me, inner)

    def there(dl, ds):
        return lax.rem(line + dl + outer, outer) * inner + lax.rem(spot + ds + inner, inner)

    peers = [lax.rem(me + k, n) for k in range(1, n)]

    def mine(i):
        return pl.ds(pl.multiple_of(i * seqs, seqs), seqs)

    my_half = pl.ds(pl.multiple_of(tp * half, half), half)
    other_half = pl.ds(pl.multiple_of((1 - tp) * half, half), half)

    def remote(src, dst, s, r, ep, core):
        return pltpu.make_async_remote_copy(
            src_ref=src, dst_ref=dst, send_sem=s, recv_sem=r, device_id=(ep, core), device_id_type=MESH)

    loads = [
        pltpu.make_async_copy(ow_hbm.at[:, pl.ds(pl.multiple_of(tp * cols, cols), cols)], ow, local.at[0]),
        pltpu.make_async_copy(gate_hbm, gate, local.at[1]),
        pltpu.make_async_copy(up_hbm, up, local.at[2]),
        pltpu.make_async_copy(down_hbm.at[:, my_half], down.at[tp], local.at[3]),
    ]
    for c in loads:
        c.start()
    barrier = pltpu.get_barrier_semaphore()
    for p in peers:
        pl.semaphore_signal(barrier, inc=1, device_id=(p, tp), device_id_type=MESH)
    pl.semaphore_signal(barrier, inc=1, device_id=(me, 1 - tp), device_id_type=MESH)
    pl.semaphore_wait(barrier, n)

    sent = []

    def begin(c):
        c.start()
        sent.append(c)
        return c

    def gather(own, view, phase, use):
        far = {dl: begin(remote(own, view(me), send.at[phase, dl * inner], recv.at[phase, dl * inner],
                                there(dl, 0), tp)) for dl in range(1, outer)}
        near = [[] for _ in range(outer)]
        for dl in range(outer):
            source = there(-dl, 0)
            if dl:
                far[dl].wait_recv()
            block = view(source) if dl else own
            for ds in range(1, inner):
                near[dl].append((dl * inner + ds, there(-dl, -ds), begin(remote(
                    block, view(source), send.at[phase, dl * inner + ds], recv.at[phase, dl * inner + ds],
                    there(0, ds), tp))))
            if dl:
                use(dl * inner, source)
        return near

    swap_down = remote(down_hbm.at[:, other_half], down.at[tp], pair_send.at[0], pair_recv.at[0], me, 1 - tp)
    begin(swap_down)
    heads[mine(me), :] = att_ref[...]
    arriving = gather(att_ref, lambda s: heads.at[mine(s)], 0, lambda k, s: None)
    gains = [begin(remote(mix_ref.at[p], mix.at[me], send.at[5, k], recv.at[5, k], p, tp))
             for k, p in enumerate(peers)]
    mix[me] = mix_ref[me]
    loads[0].wait()
    for group in arriving:
        for _, _, c in group:
            c.wait_recv()
    part[...] = lax.dot_general(heads[...], ow[...], (((1,), (1,)), ((), ())), preferred_element_type=jnp.float32)
    swap = begin(remote(part, part_in, pair_send.at[1], pair_recv.at[1], me, 1 - tp))
    swap.wait_recv()
    proj[...] = (part[...] + part_in[...]).astype(jnp.bfloat16)
    my_feats = pl.ds(pl.multiple_of(me * feats, feats), feats)
    second = [begin(remote(proj.at[mine(p)], mixed.at[:, my_feats], send.at[1, k], recv.at[1, k], p, tp))
              for k, p in enumerate(peers)]
    mixed[:, my_feats] = proj[mine(me), :]
    for c in second:
        c.wait_recv()
    residual = hid_ref[...].astype(jnp.float32) + mixed[...].astype(jnp.float32)
    resid[...] = residual
    rows[mine(me), :] = root_norm(residual, gain_ref[...]).astype(jnp.bfloat16)

    fourth = [[] for _ in range(outer)]

    def pass_on(k, s):
        fourth[k // inner].append(begin(remote(rows.at[mine(s), my_half], rows.at[mine(s), my_half],
                                   send.at[3, k], recv.at[3, k], me, 1 - tp)))

    arriving = gather(rows.at[mine(me), my_half], lambda s: rows.at[mine(s), my_half], 2, pass_on)
    near, swaps = {}, {}

    def some(dl):
        size = inner * seqs
        return pl.ds(pl.multiple_of(lax.rem(line - dl + outer, outer) * size, size), size)

    for step in range(outer + 2):
        if step < outer:
            for k, source, c in arriving[step]:
                c.wait_recv()
                pass_on(k, source)
        if step == 0:
            loads[1].wait()
            loads[2].wait()
            loads[3].wait()
            swap_down.wait_recv()
            for c in gains:
                c.wait_recv()
        dl = step - 1
        if 0 <= dl < outer:
            for c in fourth[dl]:
                c.wait_recv()
            block = rows[some(dl), :]
            gate_act = jnp.dot(block, gate[...], preferred_element_type=jnp.float32)
            up_act = jnp.dot(block, up[...], preferred_element_type=jnp.float32)
            act[tp, some(dl), :] = (gate_act / (1.0 + jnp.exp(-gate_act)) * up_act).astype(jnp.bfloat16)
            swaps[dl] = begin(remote(act.at[tp, some(dl)], act.at[tp, some(dl)],
                                     pair_send.at[4 + dl], pair_recv.at[4 + dl], me, 1 - tp))
        dl = step - 2
        if dl >= 0:
            swaps[dl].wait_recv()
            weight = mix[pl.ds(lax.rem(line - dl + outer, outer) * inner, inner)]
            eout[some(dl), :] = ((jnp.dot(act[0, some(dl), :], down[0], preferred_element_type=jnp.float32)
                                  + jnp.dot(act[1, some(dl), :], down[1], preferred_element_type=jnp.float32))
                                 * weight.reshape(inner * seqs, mix.shape[2])[:, :1]).astype(jnp.bfloat16)
            to = (outer - dl) % outer
            for ds in range(1, inner):
                k = to * inner + ds
                near[k] = begin(remote(eout.at[mine(there(to, ds))], back.at[k], send.at[4, k], recv.at[4, k],
                                       there(0, ds), tp))
    far = []
    for dl in [d for d in range(outer - 1, -1, -1)]:
        summed = eout[mine(there(dl, 0)), :].astype(jnp.float32)
        for ds in range(1, inner):
            near[dl * inner + ds].wait_recv()
            summed = summed + back[dl * inner + ds].astype(jnp.float32)
        if dl:
            sums[dl] = summed.astype(jnp.bfloat16)
            far.append((dl, begin(remote(sums.at[dl], back.at[dl * inner], send.at[4, dl * inner],
                                         recv.at[4, dl * inner], there(dl, 0), tp))))
    for dl, c in far:
        c.wait_recv()
        summed = summed + back[dl * inner].astype(jnp.float32)
    total = resid[:, my_half]
    upd[:, my_half] = (total + summed).astype(jnp.bfloat16)
    swap = begin(remote(upd.at[:, my_half], upd.at[:, my_half], pair_send.at[3], pair_recv.at[3], me, 1 - tp))
    swap.wait_recv()
    out_ref[...] = upd[...]
    for c in sent:
        c.wait_send()


def rest_kernel(attended, hidden, out_weight, ffn_gain, expert_ids, expert_scores,
                gate_weights, up_weights, down_weights):
    n = lax.axis_size("ep")
    seqs, width = hidden.shape
    cols = attended.shape[1]
    feats = out_weight.shape[0]
    units = gate_weights.shape[2]
    half = width // 2
    route_weight = expert_scores / jnp.sum(expert_scores, axis=-1, keepdims=True)
    chosen = expert_ids[None, :, :] == jnp.arange(n, dtype=jnp.int32)[:, None, None]
    mix = jnp.sum(jnp.where(chosen, route_weight[None, :, :], 0.0), axis=-1, keepdims=True)
    mix = jnp.broadcast_to(mix, (n, seqs, 128))
    bf16, f32 = jnp.bfloat16, jnp.float32
    vmem = pl.BlockSpec(memory_space=pltpu.VMEM)
    hbm = pl.BlockSpec(memory_space=pl.ANY)
    return pl.pallas_call(
        functools.partial(rest_body, n),
        out_shape=jax.ShapeDtypeStruct((seqs, width), bf16),
        in_specs=[vmem] * 4 + [hbm] * 4,
        out_specs=vmem,
        scratch_shapes=[
            pltpu.VMEM((n * seqs, cols), bf16),
            pltpu.VMEM((feats, cols), bf16),
            pltpu.VMEM((width, units), bf16),
            pltpu.VMEM((width, units), bf16),
            pltpu.VMEM((2, units, half), bf16),
            pltpu.VMEM((n * seqs, feats), f32),
            pltpu.VMEM((n * seqs, feats), f32),
            pltpu.VMEM((n * seqs, feats), bf16),
            pltpu.VMEM((seqs, width), bf16),
            pltpu.VMEM((seqs, width), f32),
            pltpu.VMEM((n * seqs, width), bf16),
            pltpu.VMEM((2, n * seqs, units), bf16),
            pltpu.VMEM((n * seqs, half), bf16),
            pltpu.VMEM((n, seqs, half), bf16),
            pltpu.VMEM((math.isqrt(n), seqs, half), bf16),
            pltpu.VMEM((n, seqs, 128), f32),
            pltpu.VMEM((seqs, width), bf16),
            pltpu.SemaphoreType.DMA((6, n)),
            pltpu.SemaphoreType.DMA((6, n)),
            pltpu.SemaphoreType.DMA((4 + math.isqrt(n),)),
            pltpu.SemaphoreType.DMA((4 + math.isqrt(n),)),
            pltpu.SemaphoreType.DMA((4,)),
        ],
        compiler_params=pltpu.CompilerParams(
            collective_id=0, has_side_effects=True, vmem_limit_bytes=60 * 1024 * 1024),
    )(attended, hidden, ffn_gain[None, :], mix, out_weight, gate_weights[0], up_weights[0], down_weights[0])


def per_device(
    hidden,
    attn_gain,
    query_weight,
    key_weight,
    value_weight,
    forget_weight,
    forget_bias,
    cache_keys,
    cache_values,
    cache_logsum,
    lengths,
    out_weight,
    ffn_gain,
    expert_ids,
    expert_scores,
    gate_weights,
    up_weights,
    down_weights,
):
    attended, key_new, value_new, new_logsum = attend(
        hidden, attn_gain, query_weight, key_weight, value_weight, forget_weight, forget_bias,
        cache_keys, cache_values, cache_logsum, lengths)
    n = lax.axis_size("ep")
    square = math.isqrt(n) ** 2 == n
    rest = rest_kernel if out_weight.shape[0] % 128 == 0 and gate_weights.shape[0] == 1 and square else rest_general
    updated = rest(attended, hidden, out_weight, ffn_gain, expert_ids, expert_scores,
                   gate_weights, up_weights, down_weights)
    return (updated, key_new, value_new, new_logsum)


def solution(mesh):
    in_specs = (
        P("ep", None),
        P(),
        P(None, "tp"),
        P(None, "tp"),
        P(None, "tp"),
        P(None, "tp"),
        P("tp"),
        P("ep", "tp", None, None),
        P("ep", "tp", None, None),
        P("ep", "tp", None),
        P("ep"),
        P("ep", None),
        P(),
        P("ep", None),
        P("ep", None),
        P("ep", None, "tp"),
        P("ep", None, "tp"),
        P("ep", "tp", None),
    )
    out_specs = (P("ep", None), P("ep", "tp", None), P("ep", "tp", None), P("ep", "tp"))
    return jax.shard_map(
        per_device, mesh=mesh, in_specs=in_specs, out_specs=out_specs, check_vma=False
    )
```

profile of v0, /device:TPU:0, one launch (start us, length us, event | category | flops | bytes accessed | tf_op | source)
XLA Modules:
  0.0 59.4 jit_solution(3063062689811247455)
XLA Ops:
  0.6 0.0 copy-start
  0.6 0.8 %convert_element_type.41 = f32[2048]{0:T(1024)S(1)} convert(bf16[2048]{0:T(1024)(128)(2,1)} %param.19) | non-fusion elementwise | flops 2048 | bytes 12288 | tf_op jit(solution)/shard_map/convert_element_type | solution.py:21
  1.5 1.0 %fusion.26 = f32[16]{0:T(128)S(1)} fusion(bf16[16,2048]{1,0:T(8,128)(2,1)} %hid_ref.1), kind=kLoop, calls=%fused_computation.23 | loop fusion | flops 98288 | bytes 65600 | tf_op jit(solution)/shard_map/reduce_sum | solution.py:20
  2.5 0.0 copy-start.1
  2.5 0.0 copy-start.2
  2.5 0.0 copy-start.11
  2.5 0.0 copy-start.12
  2.5 3.0 %convolution_convert_fusion = bf16[16,1024]{1,0:T(8,128)(2,1)S(1)} fusion(bf16[2048,1024]{1,0:T(8,128)(2,1)} %param.20, bf16[16,2048]{1,0:T(8,128)(2,1)} %hid_ref.1, f32[2048]{0:T(1024)S(1)} %convert_element_type.41, f32[16]{0:T(128)S(1)} %add_rsqrt_fusion), kind=kOutput, calls=%fused_computation.10 | convolution fusion | flops 67256320 | bytes 4300864 | tf_op jit(solution)/shard_map/dot_general | solution.py:33
  5.5 0.1 reshape.124
  5.7 0.1 iota_compare_fusion
  5.8 0.2 select_reduce_fusion
  5.9 0.0 copy-done.2
  6.0 0.0 copy-done.11
  6.0 0.2 fusion.30
  6.2 0.0 copy-start.5
  6.2 0.1 iota_compare_fusion.1
  6.3 0.0 copy-start.10
  6.3 0.0 copy-start.3
  6.3 0.0 copy-start.9
  6.4 0.5 fusion.39
  6.9 0.4 copy-done.10
  7.3 0.2 convolution_convert_fusion.2
  7.5 0.2 fusion.31
  7.7 0.3 fusion.23
  8.0 0.8 %fusion.40 = (f32[16,64]{1,0:T(8,128)S(1)}, bf16[16,64]{1,0:T(8,128)(2,1)}) fusion(bf16[2048,64]{0,1:T(8,128)(2,1)S(1)} %copy-done.3, bf16[16,2048]{1,0:T(8,128)(2,1)S(1)} %copy-done.2, f32[2048]{0:T(1024)S(1)} %convert_element_type.41, f32[16]{0:T(128)S(1)} %add_rsqrt_fusion), kind=kOutput, calls=%fused_computation.44 | convolution fusion | flops 4327424 | bytes 342080 | tf_op jit(solution)/shard_map/dot_general | solution.py:40
  8.9 0.7 %fusion.19 = bf16[16,16,64]{2,1,0:T(8,128)(2,1)S(1)} fusion(bf16[16,1,64,1024]{3,2,1,0:T(8,128)(2,1)S(1)} %copy-done.9, f32[16,16,1024]{2,1,0:T(8,128)S(1)} %get-tuple-element.7, f32[16,16]{1,0:T(8,128)S(1)} %get-tuple-element.5, f32[16,16]{1,0:T(8,128)S(1)} %multiply_maximum_fusion, f32[16,64]{1,0:T(8,128)S(1)} %get-tuple-element.8, ...), kind=kOutput, calls=%fused_computation.9 | convolution fusion | flops 34390016 | bytes 3185664 | tf_op jit(solution)/shard_map/sgjp,sgdp->sgjd/dot_general | solution.py:68
  9.6 0.0 copy-done.13
  9.6 0.7 %convert_element_type.51.att_ref = bf16[16,1024]{1,0:T(8,128)(2,1)} reshape(bf16[16,16,64]{2,1,0:T(8,128)(2,1)S(1)} %fusion.19) | data formatting | bytes 65536 | tf_op jit(solution)/shard_map/convert_element_type | solution.py:79
  10.4 0.7 %broadcast_in_dim.65.mix_ref = f32[16,16,128]{2,1,0:T(8,128)} broadcast(f32[16,16]{1,0:T(8,128)S(1)} %select_reduce_fusion.1), dimensions={0,1} | broadcast | bytes 132096 | tf_op jit(solution)/shard_map/broadcast_in_dim | solution.py:319
  11.1 0.6 %broadcast_in_dim.62.gain_ref = bf16[1,2048]{1,0:T(2,128)(2,1)} reshape(bf16[2048]{0:T(1024)(128)(2,1)S(1)} %copy-done.6) | data formatting | bytes 8192 | tf_op jit(solution)/shard_map/broadcast_in_dim | solution.py:354
  11.7 46.2 %shard_map.201 = bf16[16,2048]{1,0:T(8,128)(2,1)} custom-call(bf16[16,1024]{1,0:T(8,128)(2,1)} %convert_element_type.51.att_ref, bf16[16,2048]{1,0:T(8,128)(2,1)} %hid_ref.1, bf16[1,2048]{1,0:T(2,128)(2,1)} %broadcast_in_dim.62.gain_ref, f32[16,16,128]{2,1,0:T(8,128)} %broadcast_in_dim.65.mix_ref, bf16[128,2048]{1,0:T(8,128)(2,1)} %ow_hbm.1, ...), custom_call_target="tpu_custom_call" | custom-call | tf_op jit(solution)/shard_map/pallas_call | solution.py:323
  58.0 1.5 %copy.29 = bf16[16,2048]{1,0:T(8,128)(2,1)} copy(bf16[16,2048]{1,0:T(8,128)(2,1)} %shard_map.201) | data formatting | bytes 131072
  (22 shorter events, 0.1 us)
Async XLA Ops:
  0.6 5.7 %copy-start = (bf16[16,1,64,1024]{3,2,1,0:T(8,128)(2,1)S(1)}, bf16[16,1,64,1024]{3,2,1,0:T(8,128)(2,1)}, u32[]{:S(2)}) copy-start(bf16[16,1,64,1024]{3,2,1,0:T(8,128)(2,1)} %param.25) | copy-start | bytes 6291460
  2.5 3.2 %copy-start.8 = (s32[16]{0:T(128)S(1)}, s32[16]{0:T(128)}, u32[]{:S(2)}) copy-start(s32[16]{0:T(128)} %param.28) | copy-start | bytes 196
  2.5 3.3 %copy-start.1 = (f32[16,16,1024]{2,1,0:T(8,128)S(1)}, f32[16,16,1024]{2,1,0:T(8,128)}, u32[]{:S(2)}) copy-start(f32[16,16,1024]{2,1,0:T(8,128)} %param.27) | copy-start | bytes 3145732
  2.5 3.5 %copy-start.2 = (bf16[16,2048]{1,0:T(8,128)(2,1)S(1)}, bf16[16,2048]{1,0:T(8,128)(2,1)}, u32[]{:S(2)}) copy-start(bf16[16,2048]{1,0:T(8,128)(2,1)} %hid_ref.1) | copy-start | bytes 196612
  2.5 3.5 %copy-start.11 = (bf16[2048,16]{0,1:T(8,128)(2,1)S(1)}, bf16[2048,16]{0,1:T(8,128)(2,1)}, u32[]{:S(2)}) copy-start(bf16[2048,16]{0,1:T(8,128)(2,1)} %param.23) | copy-start | bytes 196612
  2.5 3.5 %copy-start.12 = (f32[16]{0:T(128)S(1)}, f32[16]{0:T(128)}, u32[]{:S(2)}) copy-start(f32[16]{0:T(128)} %param.24) | copy-start | bytes 196
  6.2 0.7 %copy-start.5 = (f32[16,16]{1,0:T(8,128)}, f32[16,16]{1,0:T(8,128)S(1)}, u32[]{:S(2)}) copy-start(f32[16,16]{1,0:T(8,128)S(1)} %fusion.30) | copy-start | bytes 3076
  6.3 1.0 %copy-start.10 = (bf16[2048,64]{0,1:T(8,128)(2,1)S(1)}, bf16[2048,64]{0,1:T(8,128)(2,1)}, u32[]{:S(2)}) copy-start(bf16[2048,64]{0,1:T(8,128)(2,1)} %param.21) | copy-start | bytes 786436
  6.3 1.7 %copy-start.3 = (bf16[2048,64]{0,1:T(8,128)(2,1)S(1)}, bf16[2048,64]{0,1:T(8,128)(2,1)}, u32[]{:S(2)}) copy-start(bf16[2048,64]{0,1:T(8,128)(2,1)} %param.22) | copy-start | bytes 786436
  6.3 2.5 %copy-start.9 = (bf16[16,1,64,1024]{3,2,1,0:T(8,128)(2,1)S(1)}, bf16[16,1,64,1024]{3,2,1,0:T(8,128)(2,1)}, u32[]{:S(2)}) copy-start(bf16[16,1,64,1024]{3,2,1,0:T(8,128)(2,1)} %param.26) | copy-start | bytes 6291460
  7.5 2.1 %copy-start.13 = (bf16[16,64]{1,0:T(8,128)(2,1)}, bf16[16,64]{1,0:T(8,128)(2,1)S(1)}, u32[]{:S(2)}) copy-start(bf16[16,64]{1,0:T(8,128)(2,1)S(1)} %convolution_convert_fusion.2) | copy-start | bytes 6148
  8.9 1.5 %copy-start.4 = (f32[16,6]{0,1:T(8,128)S(1)}, f32[16,6]{0,1:T(8,128)}, u32[]{:S(2)}) copy-start(f32[16,6]{0,1:T(8,128)} %param.32) | copy-start | bytes 1156
  8.9 1.5 %copy-start.7 = (s32[16,6]{0,1:T(8,128)S(1)}, s32[16,6]{0,1:T(8,128)}, u32[]{:S(2)}) copy-start(s32[16,6]{0,1:T(8,128)} %param.31) | copy-start | bytes 1156
  8.9 2.3 %copy-start.6 = (bf16[2048]{0:T(1024)(128)(2,1)S(1)}, bf16[2048]{0:T(1024)(128)(2,1)}, u32[]{:S(2)}) copy-start(bf16[2048]{0:T(1024)(128)(2,1)} %param.30) | copy-start | bytes 12292
where the time goes:
time: 59.7 us; the launch traced here: 59.4 us
  Pallas kernels  46.2 us (77%)
  matrix products  5.67 us (9%)
  local copies, waits for them, and re-layouts  4.14 us (7%)
  other arithmetic  2.54 us (4%)
  between operations  0.86 us (1%)
    pallas_call x1, Pallas kernels, rest_kernel(): pl.pallas_call(functools.partial(rest_body, n), out_shape=jax.ShapeDtypeS...  46.2 us
    dot_general x1, matrix products, attend(): jnp.dot(normed, query_weight, preferred_element_type=jnp.float32)  3.01 us
    unnamed x29, local copies, waits for them, and re-layouts  1.95 us

commit v1 on v0

v1 whole, which is shorter than its diff:
```python
import functools
import math

import jax
import jax.numpy as jnp
from jax import lax
from jax.experimental import pallas as pl
from jax.experimental.pallas import tpu as pltpu
from jax.sharding import PartitionSpec as P

HD = 64
TOP_K = 6


epsilon = 1e-06


def root_norm(values_in, gain):
    floats = values_in.astype(jnp.float32)
    inv_root = lax.rsqrt(jnp.mean(floats * floats, axis=-1, keepdims=True) + epsilon)
    return floats * inv_root * gain.astype(jnp.float32)


def attend(hidden, attn_gain, query_weight, key_weight, value_weight, forget_weight, forget_bias,
           cache_keys, cache_values, cache_logsum, lengths):
    rows_here = hidden.shape[0]
    query_heads = query_weight.shape[1] // HD
    key_heads = key_weight.shape[1] // HD
    group_size = query_heads // key_heads
    cache_len = cache_keys.shape[-1]
    score_scale = HD ** (-0.5)
    normed = root_norm(hidden, attn_gain).astype(jnp.bfloat16)
    queries = jnp.dot(normed, query_weight, preferred_element_type=jnp.float32).astype(jnp.bfloat16)
    key_new = (
        jnp.dot(normed, key_weight, preferred_element_type=jnp.float32)
        .astype(jnp.bfloat16)
        .reshape(rows_here, key_heads, HD)
    )
    value_new = (
        jnp.dot(normed, value_weight, preferred_element_type=jnp.float32)
        .astype(jnp.bfloat16)
        .reshape(rows_here, key_heads, HD)
    )
    log_forget = jax.nn.log_sigmoid(
        jnp.dot(normed, forget_weight, preferred_element_type=jnp.float32) + forget_bias
    )
    positions = jnp.arange(cache_len, dtype=jnp.int32)
    is_last = positions[None, :] == (lengths - 1)[:, None]
    new_logsum = jnp.sum(jnp.where(is_last[:, None, :], cache_logsum, 0.0), axis=-1) + log_forget
    grouped = queries.reshape(rows_here, key_heads, group_size, HD)
    scores = jnp.einsum("sgjd,sgdp->sgjp", grouped, cache_keys, preferred_element_type=jnp.float32)
    scores = scores.reshape(rows_here, query_heads, cache_len) * score_scale
    scores = scores + new_logsum[:, :, None] - cache_logsum
    is_live = positions[None, :] < lengths[:, None]
    scores = jnp.where(is_live[:, None, :], scores, -jnp.inf)
    own_score = (
        jnp.einsum("sgjd,sgd->sgj", grouped, key_new, preferred_element_type=jnp.float32).reshape(
            rows_here, query_heads
        )
        * score_scale
    )
    top_score = jnp.maximum(jnp.max(scores, axis=-1), own_score)
    past_exp = jnp.exp(scores - top_score[:, :, None])
    own_exp = jnp.exp(own_score - top_score)
    denominator = jnp.sum(past_exp, axis=-1) + own_exp
    past_weight = (past_exp / denominator[:, :, None]).astype(jnp.bfloat16)
    own_weight = (own_exp / denominator).astype(jnp.bfloat16)
    attended = jnp.einsum(
        "sgjp,sgdp->sgjd",
        past_weight.reshape(rows_here, key_heads, group_size, cache_len),
        cache_values,
        preferred_element_type=jnp.float32,
    )
    attended = (
        attended
        + own_weight.astype(jnp.float32).reshape(rows_here, key_heads, group_size)[:, :, :, None]
        * value_new.astype(jnp.float32)[:, :, None, :]
    )
    attended = attended.reshape(rows_here, query_heads * HD).astype(jnp.bfloat16)
    return attended, key_new, value_new, new_logsum


def rest_general(attended, hidden, out_weight, ffn_gain, expert_ids, expert_scores,
                 gate_weights, up_weights, down_weights):
    rows_here = hidden.shape[0]
    whole_heads = lax.all_gather(attended, "tp", axis=1, tiled=True)
    projected = lax.dot_general(
        lax.all_gather(whole_heads, "ep", axis=0, tiled=True),
        out_weight,
        (((1,), (1,)), ((), ())),
        preferred_element_type=jnp.float32,
    ).astype(jnp.bfloat16)
    mixed = lax.all_to_all(projected, "ep", split_axis=0, concat_axis=1, tiled=True)
    residual = hidden.astype(jnp.float32) + mixed.astype(jnp.float32)
    ffn_in = root_norm(residual, ffn_gain).astype(jnp.bfloat16)
    ep_size = lax.axis_size("ep")
    local_experts = gate_weights.shape[0]
    experts = ep_size * local_experts
    route_count = rows_here * TOP_K
    capacity = 2 * ((route_count + experts - 1) // experts)
    flat_ids = expert_ids.reshape(route_count)
    onehot = (flat_ids[:, None] == jnp.arange(experts, dtype=jnp.int32)[None, :]).astype(jnp.int32)
    running = jnp.cumsum(onehot, axis=0)
    slot_index = jnp.sum(running * onehot, axis=1) - 1
    target = flat_ids * capacity + slot_index
    dispatch_map = (
        target[:, None] == jnp.arange(experts * capacity, dtype=jnp.int32)[None, :]
    ).astype(jnp.bfloat16)
    route_rows = jnp.repeat(ffn_in, TOP_K, axis=0)
    outgoing = lax.dot_general(
        dispatch_map, route_rows, (((0,), (0,)), ((), ())), preferred_element_type=jnp.float32
    )
    outgoing = outgoing.astype(jnp.bfloat16).reshape(
        ep_size, local_experts, capacity, ffn_in.shape[1]
    )
    arrived = lax.all_to_all(outgoing, "ep", split_axis=0, concat_axis=0, tiled=True)
    gate_act = jnp.einsum(
        "sekd,edf->sekf", arrived, gate_weights, preferred_element_type=jnp.float32
    )
    up_act = jnp.einsum("sekd,edf->sekf", arrived, up_weights, preferred_element_type=jnp.float32)
    hidden_act = (jax.nn.silu(gate_act) * up_act).astype(jnp.bfloat16)
    partial_out = jnp.einsum(
        "sekf,efd->sekd", hidden_act, down_weights, preferred_element_type=jnp.float32
    )
    half_sum = lax.psum_scatter(
        partial_out.astype(jnp.bfloat16), "tp", scatter_dimension=3, tiled=True
    )
    sent_back = lax.all_to_all(half_sum, "ep", split_axis=0, concat_axis=0, tiled=True)
    share_width = sent_back.shape[-1]
    picked = jnp.dot(
        dispatch_map,
        sent_back.reshape(experts * capacity, share_width),
        preferred_element_type=jnp.float32,
    )
    route_weight = expert_scores / jnp.sum(expert_scores, axis=-1, keepdims=True)
    expert_mix = jnp.sum(
        picked.reshape(rows_here, TOP_K, share_width) * route_weight[:, :, None], axis=1
    )
    own_part = lax.dynamic_slice_in_dim(
        residual, lax.axis_index("tp") * share_width, share_width, 1
    )
    updated = lax.all_gather((own_part + expert_mix).astype(jnp.bfloat16), "tp", axis=1, tiled=True)
    return updated


MESH = pl.DeviceIdType.MESH
PLANE = 4


def step_body(n, len_ref, fbias_ref, hid_ref, again_ref, fgain_ref, ids_ref, rscore_ref,
              qw_hbm, kw_hbm, vw_hbm, fw_hbm, keys_hbm, vals_hbm, logs_hbm, ow_hbm, gate_hbm, up_hbm, down_hbm,
              out_ref, key_ref, val_ref, nlog_ref,
              qw, kw, vw, fw, keys, vals, logs, scores, maxes, lasts, sums, mixed_heads, att, ow, gate, up, down,
              hidl, psend, pin, mixl, mixin, rows, ssq, wts, gacc, uacc, act, eout, back, fsum, far, upd,
              send, recv, local):
    f32, bf16 = jnp.float32, jnp.bfloat16
    me, tp = lax.axis_index("ep"), lax.axis_index("tp")
    seqs, width = hid_ref.shape
    cols = qw.shape[1]
    heads = cols // HD
    cache_len = keys.shape[2]
    outer = n // PLANE
    feats = ow.shape[1]
    pf = PLANE * feats
    xq = pf // 2
    line = outer * seqs
    z, xy = me // PLANE, lax.rem(me, PLANE)
    x, y = lax.rem(xy, 2), xy // 2
    spots = [y * 2 + (1 - x), (1 - y) * 2 + x, (1 - y) * 2 + (1 - x)]
    plane = [z * PLANE + s for s in spots]

    def zdev(zz):
        return zz * PLANE + xy

    near_tables = [sorted([j for j in range(outer) if j != i], key=lambda j: (abs(j - i), j)) for i in range(outer)]

    def nth(k):
        value = near_tables[0][k]
        for i in range(1, outer):
            value = jnp.where(z == i, near_tables[i][k], value)
        return value

    zs = [nth(k) for k in range(outer - 1)]
    used = {"s": 0, "r": 0, "l": 0}

    def take(kind, count=1):
        base = used[kind]
        used[kind] += count
        return base

    sent = []

    def copy(src, dst, s, r, ep, core):
        return pltpu.make_async_remote_copy(src_ref=src, dst_ref=dst, send_sem=send.at[s], recv_sem=recv.at[r],
                                            device_id=(ep, core), device_id_type=MESH)

    def begin(src, dst, r, ep, core):
        c = copy(src, dst, take("s"), r, ep, core)
        c.start()
        sent.append(c)
        return c

    def arrived(dst, r):
        copy(dst, dst, 0, r, me, 1 - tp).wait_recv()

    def load(src, dst):
        c = pltpu.make_async_copy(src, dst, local.at[take("l")])
        c.start()
        return c

    def sl(i, size):
        return pl.ds(pl.multiple_of(i * size, size), size)

    ow_load = load(ow_hbm.at[:, sl(tp, cols)], ow.at[xy])
    small = [load(kw_hbm, kw), load(vw_hbm, vw), load(fw_hbm, fw)]
    qchunk = width // 4
    qw_loads = [load(qw_hbm.at[pl.ds(i * qchunk, qchunk)], qw.at[pl.ds(i * qchunk, qchunk)]) for i in range(4)]
    part = seqs // 4
    key_loads = [load(keys_hbm.at[pl.ds(i * part, part), 0], keys.at[pl.ds(i * part, part)]) for i in range(4)]
    log_loads = [load(logs_hbm.at[pl.ds(i * part, part)], logs.at[pl.ds(i * part, part)]) for i in range(4)]
    val_loads = [load(vals_hbm.at[pl.ds(i * part, part), 0], vals.at[pl.ds(i * part, part)]) for i in range(4)]

    barrier = pltpu.get_barrier_semaphore()
    for d in range(1, outer):
        pl.semaphore_signal(barrier, inc=1, device_id=(zdev(lax.rem(z + d, outer)), tp), device_id_type=MESH)
    for p in plane:
        pl.semaphore_signal(barrier, inc=1, device_id=(p, tp), device_id_type=MESH)
    pl.semaphore_signal(barrier, inc=1, device_id=(me, 1 - tp), device_id_type=MESH)

    normed = root_norm(hid_ref[...], again_ref[...]).astype(bf16)
    rscore = rscore_ref[...]
    route = rscore / jnp.sum(rscore, axis=-1, keepdims=True)
    lanes = lax.broadcasted_iota(jnp.int32, (seqs, 128), 1)
    table = jnp.zeros((seqs, 128), f32)
    for k in range(TOP_K):
        table = table + jnp.where(lanes == ids_ref[:, k:k + 1], route[:, k:k + 1], 0.0)
    wts[xy, sl(z, seqs), :] = table

    pl.semaphore_wait(barrier, outer - 1 + 3 + 1)

    hf = feats // 2
    lo, hi = pl.ds(0, hf), pl.ds(hf, hf)
    ow_load.wait()
    ow_r = take("r", 6)
    begin(ow.at[xy, lo], ow.at[xy, lo], ow_r, plane[0], tp)
    begin(ow.at[xy, hi], ow.at[xy, hi], ow_r + 3, plane[1], tp)
    begin(ow.at[xy, hi], ow.at[xy, hi], ow_r + 1, plane[0], tp)
    begin(ow.at[xy, lo], ow.at[xy, lo], ow_r + 2, plane[1], tp)
    hid_r = take("r", outer)
    for zz in zs:
        begin(hid_ref.at[:, pl.ds(pl.multiple_of(zz * pf + tp * xq, xq), xq)], hidl.at[sl(z, seqs)],
              hid_r + z, zdev(zz), tp)
    hidl[sl(z, seqs), :] = hid_ref[:, pl.ds(pl.multiple_of(z * pf + tp * xq, xq), xq)]
    wt_r = take("r", outer)
    for zz in zs:
        begin(wts.at[xy, sl(z, seqs)], wts.at[xy, sl(z, seqs)], wt_r + z, zdev(zz), tp)

    acc = jnp.zeros((seqs, cols), f32)
    for i in range(4):
        qw_loads[i].wait()
        acc = acc + jnp.dot(normed[:, i * qchunk:(i + 1) * qchunk], qw[pl.ds(i * qchunk, qchunk), :],
                            preferred_element_type=f32)
    queries = acc.astype(bf16).astype(f32) * (HD ** -0.5)
    for c in small:
        c.wait()
    key_new = jnp.dot(normed, kw[...], preferred_element_type=f32).astype(bf16)
    value_new = jnp.dot(normed, vw[...], preferred_element_type=f32).astype(bf16)
    key_ref[...] = key_new
    val_ref[...] = value_new
    hl = lax.broadcasted_iota(jnp.int32, (seqs, heads), 1)
    fb = jnp.zeros((seqs, heads), f32)
    for h in range(heads):
        fb = jnp.where(hl == h, fbias_ref[h], fb)
    pre = jnp.dot(normed, fw[...], preferred_element_type=f32) + fb
    log_forget = jnp.minimum(pre, 0.0) - jnp.log1p(jnp.exp(-jnp.abs(pre)))

    gate_loads, up_loads = [], []
    for t in range(2):
        for zc in range(outer):
            rows_from = pl.ds(zc * pf + t * xq, xq)
            gate_loads.append(load(gate_hbm.at[0, rows_from], gate.at[t * outer + zc]))
            up_loads.append(load(up_hbm.at[0, rows_from], up.at[t * outer + zc]))
    down_loads, down_r = [], take("r", outer)
    for zc in range(outer):
        mine = pl.ds(pl.multiple_of(zc * pf + tp * xq, xq), xq)
        other = pl.ds(pl.multiple_of(zc * pf + (1 - tp) * xq, xq), xq)
        down_loads.append(load(down_hbm.at[0, :, mine], down.at[tp, :, pl.ds(zc * xq, xq)]))
        begin(down_hbm.at[0, :, other], down.at[tp, :, pl.ds(zc * xq, xq)], down_r + zc, me, 1 - tp)

    total = seqs * heads

    def spread(v):
        return jnp.broadcast_to(v[:, None, :], (seqs, heads, v.shape[1])).reshape(total, v.shape[1])

    row_head = lax.rem(lax.broadcasted_iota(jnp.int32, (total, 128), 0), heads)
    picked = jnp.zeros((total, 128), f32)
    for j in range(cols // 128):
        picked = jnp.where(row_head // 2 == j, spread(queries[:, j * 128:(j + 1) * 128]), picked)
    picked = jnp.where(lax.rem(row_head, 2) == 0, picked, pltpu.roll(picked, HD, 1))[:, :HD]
    per_head = picked.astype(bf16)
    own = jnp.sum(picked * spread(key_new.astype(f32)), axis=-1, keepdims=True)

    positions = lax.broadcasted_iota(jnp.int32, (heads, cache_len), 1)
    for s in range(seqs):
        if s % part == 0:
            key_loads[s // part].wait()
            log_loads[s // part].wait()
        here = pl.ds(s * heads, heads)
        size = len_ref[s]
        level = logs[s]
        dots = jnp.dot(per_head[s * heads:(s + 1) * heads, :], keys[s], preferred_element_type=f32)
        past = jnp.where(positions < size, dots - level, -jnp.inf)
        scores[here, :] = past
        maxes[here, :] = jnp.broadcast_to(jnp.max(past, axis=-1, keepdims=True), (heads, 128))
        last = jnp.sum(jnp.where(positions == size - 1, level, 0.0), axis=-1, keepdims=True)
        lasts[here, :] = jnp.broadcast_to(last, (heads, 128))
    own_lane = lax.broadcasted_iota(jnp.int32, (total, heads), 1)
    own_row = lax.rem(lax.broadcasted_iota(jnp.int32, (total, heads), 0), heads)
    forget_col = jnp.sum(jnp.where(own_lane == own_row, spread(log_forget), 0.0), axis=-1, keepdims=True)
    newlog = lasts[:, :1] + forget_col
    nlog_ref[...] = jnp.sum(jnp.where(own_lane == own_row, jnp.broadcast_to(newlog, (total, heads)), 0.0)
                            .reshape(seqs, heads, heads), axis=1)
    own = own - newlog
    peak = jnp.maximum(maxes[:, :1], own)
    maxes[...] = jnp.broadcast_to(peak, (total, 128))
    for s in range(seqs):
        if s % part == 0:
            val_loads[s // part].wait()
        here = pl.ds(s * heads, heads)
        weights = jnp.exp(scores[here, :] - maxes[here, :][:, :1])
        sums[here, :] = jnp.broadcast_to(jnp.sum(weights, axis=-1, keepdims=True), (heads, 128))
        mixed_heads[here, :HD] = lax.dot_general(weights.astype(bf16), vals[s], (((1,), (1,)), ((), ())),
                                                 preferred_element_type=f32)
    own_exp = jnp.exp(own - peak)
    inverse = 1.0 / (sums[:, :1] + own_exp)
    outs = (mixed_heads[:, :HD] + own_exp * spread(value_new.astype(f32))) * inverse
    mixed_heads[:, :HD] = outs
    mixed_heads[:, HD:] = outs
    wide = lax.broadcasted_iota(jnp.int32, (seqs, 128), 1)
    for j in range(cols // 128):
        even = mixed_heads[pl.ds(2 * j, seqs, stride=heads), :]
        odd = mixed_heads[pl.ds(2 * j + 1, seqs, stride=heads), :]
        att[sl(z, seqs), j * 128:(j + 1) * 128] = jnp.where(wide < HD, even, odd).astype(bf16)

    att_r = take("r", outer)
    for zz in reversed(zs):
        begin(att.at[sl(z, seqs)], att.at[sl(z, seqs)], att_r + z, zdev(zz), tp)
    arrived(ow.at[spots[0], lo], ow_r)
    relay_r = take("r", 2)
    begin(ow.at[spots[0], lo], ow.at[spots[0], lo], relay_r, plane[1], tp)
    arrived(ow.at[spots[1], hi], ow_r + 3)
    begin(ow.at[spots[1], hi], ow.at[spots[1], hi], relay_r + 1, plane[0], tp)
    for zz in zs:
        arrived(wts.at[xy, sl(zz, seqs)], wt_r + zz)
    wline_r = take("r", 3)
    for i in range(3):
        begin(wts.at[xy], wts.at[xy], wline_r + i, plane[i], tp)
    arrived(ow.at[spots[0], hi], ow_r + 1)
    arrived(ow.at[spots[1], lo], ow_r + 2)
    for zz in zs:
        arrived(hidl.at[sl(zz, seqs)], hid_r + zz)
    for zz in zs:
        arrived(att.at[sl(zz, seqs)], att_r + zz)
    arrived(ow.at[spots[2], lo], relay_r)
    arrived(ow.at[spots[2], hi], relay_r + 1)
    lines = att[...]

    def project(t):
        return [lax.dot_general(lines, ow[2 * t + i], (((1,), (1,)), ((), ())), preferred_element_type=f32)
                for i in range(2)]

    for i, v in enumerate(project(1 - tp)):
        psend[:, i * feats:(i + 1) * feats] = v
    p_r = take("r")
    begin(psend, pin, p_r, me, 1 - tp)
    kept = jnp.concatenate(project(tp), axis=1)
    arrived(pin, p_r)
    mixed = (kept + pin[...]).astype(bf16)
    residual = hidl[...].astype(f32) + mixed.astype(f32)
    gain = fgain_ref[:, pl.ds(pl.multiple_of(z * pf + tp * xq, xq), xq)].astype(f32)
    block = tp * outer + z
    rows[block, xy] = (residual * gain).astype(bf16)
    square = jnp.sum(residual * residual, axis=-1, keepdims=True)
    eye = (lax.broadcasted_iota(jnp.int32, (line, line), 0) == lax.broadcasted_iota(jnp.int32, (line, line), 1))
    flat = jnp.sum(jnp.where(eye, jnp.broadcast_to(square, (line, line)), 0.0), axis=0, keepdims=True)
    ssq[block, xy] = jnp.broadcast_to(flat, (8, line))
    mixl[...] = mixed

    zrow_r, zsq_r = take("r", outer), take("r", outer)
    prow_r, psq_r = take("r", 3 * outer), take("r", 3 * outer)
    crow_r, csq_r = take("r", 4 * outer), take("r", 4 * outer)

    def out_to_plane(zz):
        b = tp * outer + zz
        for i in range(3):
            begin(rows.at[b, xy], rows.at[b, xy], prow_r + i * outer + zz, plane[i], tp)
            begin(ssq.at[b, xy], ssq.at[b, xy], psq_r + i * outer + zz, plane[i], tp)

    def to_partner(zz, i, spot):
        b = tp * outer + zz
        begin(rows.at[b, spot], rows.at[b, spot], crow_r + i * outer + zz, me, 1 - tp)
        begin(ssq.at[b, spot], ssq.at[b, spot], csq_r + i * outer + zz, me, 1 - tp)

    for zz in reversed(zs):
        begin(rows.at[block, xy], rows.at[block, xy], zrow_r + z, zdev(zz), tp)
        begin(ssq.at[block, xy], ssq.at[block, xy], zsq_r + z, zdev(zz), tp)
    out_to_plane(z)
    to_partner(z, 3, xy)
    mix_r = take("r", outer)
    for zz in zs:
        begin(mixl.at[sl(zz, seqs)], mixin.at[z], mix_r + z, zdev(zz), tp)
    mixin[z] = mixl[sl(z, seqs), :]
    for zz in zs:
        b = tp * outer + zz
        arrived(rows.at[b, xy], zrow_r + zz)
        arrived(ssq.at[b, xy], zsq_r + zz)
        out_to_plane(zz)
        to_partner(zz, 3, xy)
    for c in gate_loads + up_loads + down_loads:
        c.wait()
    for i in range(3):
        arrived(wts.at[spots[i]], wline_r + i)

    def gather_block(t, zz, first):
        b = t * outer + zz
        left = rows[b].reshape(PLANE * line, xq)
        g = jnp.dot(left, gate[b], preferred_element_type=f32)
        u = jnp.dot(left, up[b], preferred_element_type=f32)
        gacc[...] = g if first else gacc[...] + g
        uacc[...] = u if first else uacc[...] + u

    order = [z] + zs
    for k in range(outer + 1):
        if k < outer:
            b = tp * outer + order[k]
            for i in range(3):
                arrived(rows.at[b, spots[i]], prow_r + i * outer + order[k])
                arrived(ssq.at[b, spots[i]], psq_r + i * outer + order[k])
                to_partner(order[k], i, spots[i])
            gather_block(tp, order[k], k == 0)
        if k > 0:
            b = (1 - tp) * outer + order[k - 1]
            for i, spot in enumerate(spots + [xy]):
                arrived(rows.at[b, spot], crow_r + i * outer + order[k - 1])
                arrived(ssq.at[b, spot], csq_r + i * outer + order[k - 1])
            gather_block(1 - tp, order[k - 1], False)
    for q in range(PLANE):
        whole = ssq[0, q][:1, :]
        for b in range(1, 2 * outer):
            whole = whole + ssq[b, q][:1, :]
        scale = lax.rsqrt(whole * (1.0 / width) + epsilon)
        scale = jnp.sum(jnp.where(eye, jnp.broadcast_to(scale, (line, line)), 0.0), axis=1, keepdims=True)
        g = gacc[pl.ds(q * line, line), :] * scale
        u = uacc[pl.ds(q * line, line), :] * scale
        act[tp, q] = (g / (1.0 + jnp.exp(-g)) * u).astype(bf16)
    act_r = take("r")
    begin(act.at[tp], act.at[tp], act_r, me, 1 - tp)
    for zc in range(outer):
        arrived(down.at[1 - tp, :, pl.ds(zc * xq, xq)], down_r + zc)
    arrived(act.at[1 - tp], act_r)

    back_r = take("r", 3 * outer)
    out_order = list(reversed(zs)) + [z]
    which = lax.broadcasted_iota(jnp.int32, (PLANE * seqs, 128), 1) == me
    for zz in out_order:
        def tokens(ref):
            return ref[:, sl(zz, seqs), :].reshape(PLANE * seqs, ref.shape[2])

        weight = jnp.sum(jnp.where(which, tokens(wts), 0.0), axis=-1, keepdims=True)
        made = (jnp.dot(tokens(act.at[0]), down[0], preferred_element_type=f32)
                + jnp.dot(tokens(act.at[1]), down[1], preferred_element_type=f32)) * weight
        eout[zz] = made.astype(bf16).reshape(PLANE, seqs, made.shape[1])
        for i in (2, 0, 1):
            begin(eout.at[zz, spots[i]], back.at[i, zz], back_r + i * outer + zz, plane[i], tp)
    far_r = take("r", outer)
    for zz in out_order:
        summed = eout[zz, xy].astype(f32)
        for i in range(3):
            arrived(back.at[i, zz], back_r + i * outer + zz)
            summed = summed + back[i, zz].astype(f32)
        if zz is not z:
            fsum[zz] = summed.astype(bf16)
            begin(fsum.at[zz], far.at[z], far_r + z, zdev(zz), tp)
    for zz in zs:
        arrived(mixin.at[zz], mix_r + zz)
    for zz in zs:
        arrived(far.at[zz], far_r + zz)
        summed = summed + far[zz].astype(f32)
    for zc in range(outer):
        here = hid_ref[:, pl.ds(pl.multiple_of(zc * pf + tp * xq, xq), xq)].astype(f32) + mixin[zc].astype(f32)
        upd[tp, :, zc * xq:(zc + 1) * xq] = (here + summed[:, zc * xq:(zc + 1) * xq]).astype(bf16)
    u_r = take("r")
    begin(upd.at[tp], upd.at[tp], u_r, me, 1 - tp)
    arrived(upd.at[1 - tp], u_r)
    for t in range(2):
        for zc in range(outer):
            out_ref[:, zc * pf + t * xq:zc * pf + (t + 1) * xq] = upd[t, :, zc * xq:(zc + 1) * xq]
    for c in sent:
        c.wait_send()
    assert used["s"] <= send.shape[0] and used["r"] <= recv.shape[0] and used["l"] <= local.shape[0], used


def step_kernel(hidden, attn_gain, query_weight, key_weight, value_weight, forget_weight, forget_bias,
                cache_keys, cache_values, cache_logsum, lengths, out_weight, ffn_gain, expert_ids, expert_scores,
                gate_weights, up_weights, down_weights):
    n = lax.axis_size("ep")
    seqs, width = hidden.shape
    cols = query_weight.shape[1]
    heads = cols // HD
    cache_len = cache_keys.shape[3]
    feats = out_weight.shape[0]
    units = gate_weights.shape[2]
    outer = n // PLANE
    line = outer * seqs
    xq = PLANE * feats // 2
    half = width // 2
    bf16, f32 = jnp.bfloat16, jnp.float32
    vmem = pl.BlockSpec(memory_space=pltpu.VMEM)
    smem = pl.BlockSpec(memory_space=pltpu.SMEM)
    hbm = pl.BlockSpec(memory_space=pl.ANY)
    v = pltpu.VMEM
    updated, key_new, value_new, new_logsum = pl.pallas_call(
        functools.partial(step_body, n),
        out_shape=[jax.ShapeDtypeStruct((seqs, width), bf16), jax.ShapeDtypeStruct((seqs, HD), bf16),
                   jax.ShapeDtypeStruct((seqs, HD), bf16), jax.ShapeDtypeStruct((seqs, heads), f32)],
        in_specs=[smem] * 2 + [vmem] * 5 + [hbm] * 11,
        out_specs=[vmem] * 4,
        scratch_shapes=[
            v((width, cols), bf16), v((width, HD), bf16), v((width, HD), bf16), v((width, heads), bf16),
            v((seqs, HD, cache_len), bf16), v((seqs, HD, cache_len), bf16), v((seqs, heads, cache_len), f32),
            v((seqs * heads, cache_len), f32), v((seqs * heads, 128), f32), v((seqs * heads, 128), f32),
            v((seqs * heads, 128), f32), v((seqs * heads, 2 * HD), f32),
            v((line, cols), bf16), v((PLANE, feats, cols), bf16),
            v((2 * outer, xq, units), bf16), v((2 * outer, xq, units), bf16), v((2, units, half), bf16),
            v((line, xq), bf16), v((line, xq), f32), v((line, xq), f32), v((line, xq), bf16),
            v((outer, seqs, xq), bf16),
            v((2 * outer, PLANE, line, xq), bf16), v((2 * outer, PLANE, 8, line), f32), v((PLANE, line, 128), f32),
            v((PLANE * line, units), f32), v((PLANE * line, units), f32), v((2, PLANE, line, units), bf16),
            v((outer, PLANE, seqs, half), bf16), v((3, outer, seqs, half), bf16),
            v((outer, seqs, half), bf16), v((outer, seqs, half), bf16), v((2, seqs, half), bf16),
            pltpu.SemaphoreType.DMA((200,)), pltpu.SemaphoreType.DMA((200,)), pltpu.SemaphoreType.DMA((64,)),
        ],
        compiler_params=pltpu.CompilerParams(
            collective_id=0, has_side_effects=True, vmem_limit_bytes=60 * 1024 * 1024),
    )(lengths, forget_bias, hidden, attn_gain[None, :], ffn_gain[None, :], expert_ids, expert_scores,
      query_weight, key_weight, value_weight, forget_weight, cache_keys, cache_values, cache_logsum,
      out_weight, gate_weights, up_weights, down_weights)
    return updated, key_new.reshape(seqs, 1, HD), value_new.reshape(seqs, 1, HD), new_logsum


def per_device(hidden, attn_gain, query_weight, key_weight, value_weight, forget_weight, forget_bias,
               cache_keys, cache_values, cache_logsum, lengths, out_weight, ffn_gain, expert_ids, expert_scores,
               gate_weights, up_weights, down_weights):
    n = lax.axis_size("ep")
    seqs, width = hidden.shape
    fits = (
        n % PLANE == 0
        and lax.axis_size("tp") == 2
        and gate_weights.shape[0] == 1
        and cache_keys.shape[1] == 1
        and seqs % 16 == 0
        and (query_weight.shape[1] // HD) % 16 == 0
        and out_weight.shape[0] % 128 == 0
        and n <= 128
    )
    if fits:
        return step_kernel(
            hidden, attn_gain, query_weight, key_weight, value_weight, forget_weight, forget_bias,
            cache_keys, cache_values, cache_logsum, lengths, out_weight, ffn_gain, expert_ids, expert_scores,
            gate_weights, up_weights, down_weights)
    attended, key_new, value_new, new_logsum = attend(
        hidden, attn_gain, query_weight, key_weight, value_weight, forget_weight, forget_bias,
        cache_keys, cache_values, cache_logsum, lengths)
    updated = rest_general(attended, hidden, out_weight, ffn_gain, expert_ids, expert_scores,
                           gate_weights, up_weights, down_weights)
    return (updated, key_new, value_new, new_logsum)


def solution(mesh):
    in_specs = (
        P("ep", None),
        P(),
        P(None, "tp"),
        P(None, "tp"),
        P(None, "tp"),
        P(None, "tp"),
        P("tp"),
        P("ep", "tp", None, None),
        P("ep", "tp", None, None),
        P("ep", "tp", None),
        P("ep"),
        P("ep", None),
        P(),
        P("ep", None),
        P("ep", None),
        P("ep", None, "tp"),
        P("ep", None, "tp"),
        P("ep", "tp", None),
    )
    out_specs = (P("ep", None), P("ep", "tp", None), P("ep", "tp", None), P("ep", "tp"))
    return jax.shard_map(
        per_device, mesh=mesh, in_specs=in_specs, out_specs=out_specs, check_vma=False
    )
```

time: 59.7 us -> 66 us (1.11)
  local copies, waits for them, and re-layouts: 4.14 us -> 16.4 us
  matrix products: 5.67 us -> 0 us
  other arithmetic: 2.54 us -> 0 us
  Pallas kernels: 46.2 us -> 48.4 us
    unnamed x29 -> x9, local copies, waits for them, and re-layouts: 1.95 us -> 13.8 us
    dot_general x7 -> x0, matrix products: 5.67 us -> none  [the longest x1 3.01 us: attend(): jnp.dot(normed, query_weight, preferred_element_type=jnp.float32)]
    pallas_call x1, Pallas kernels: 46.2 us -> 48.4 us  [step_kernel(): pl.pallas_call(functools.partial(step_body, n), out_shape=[jax.ShapeDtype...]
    reduce_sum x5 -> x0, other arithmetic: 1.5 us -> none  [the longest x1 0.97 us: root_norm(): jnp.mean(floats * floats, axis=-1, keepdims=True) + epsilon]
    broadcast_in_dim x2, local copies, waits for them, and re-layouts: 1.34 us -> 2.58 us  [the longest x1 1.29 us: step_kernel(): attn_gain[None, :]]
    convert_element_type x2 -> x0, other arithmetic: 0.85 us -> none  [the longest x1 0.84 us: root_norm(): return floats * inv_root * gain.astype(jnp.float32)]
    convert_element_type x1 -> x0, local copies, waits for them, and re-layouts: 0.74 us -> none  [attend(): attended.reshape(rows_here, query_heads * HD).astype(jnp.bfloat16)]
where the time goes in v1:
time: 66 us; the launch traced here: 65.5 us
  Pallas kernels  48.4 us (73%)
  local copies, waits for them, and re-layouts  16.4 us (25%)
    pallas_call x1, Pallas kernels, step_kernel(): pl.pallas_call(functools.partial(step_body, n), out_shape=[jax.ShapeDtype...  48.4 us
    unnamed x9, local copies, waits for them, and re-layouts  13.8 us

profile of v1, /device:TPU:0, one launch (start us, length us, event | category | flops | bytes accessed | tf_op | source)
XLA Modules:
  0.0 65.5 jit_solution(1954123026014275392)
XLA Ops:
  0.6 1.3 %broadcast_in_dim.6.again_ref = bf16[1,2048]{1,0:T(2,128)(2,1)} reshape(bf16[2048]{0:T(1024)(128)(2,1)} %param.19) | data formatting | bytes 8192 | tf_op jit(solution)/shard_map/broadcast_in_dim | solution.py:545
  1.9 1.3 %broadcast_in_dim.7.fgain_ref = bf16[1,2048]{1,0:T(2,128)(2,1)} reshape(bf16[2048]{0:T(1024)(128)(2,1)} %param.30) | data formatting | bytes 8192 | tf_op jit(solution)/shard_map/broadcast_in_dim | solution.py:545
  3.2 1.4 %copy.22.ids_ref = s32[16,6]{1,0:T(8,128)} copy(s32[16,6]{0,1:T(8,128)} %param.31) | data formatting | bytes 768 | tf_op args[13]
  4.6 1.4 %copy.23.rscore_ref = f32[16,6]{1,0:T(8,128)} copy(f32[16,6]{0,1:T(8,128)} %param.32) | data formatting | bytes 768 | tf_op args[14]
  5.9 1.9 %copy.24.kw_hbm = bf16[2048,64]{1,0:T(8,128)(2,1)} copy(bf16[2048,64]{0,1:T(8,128)(2,1)} %param.21) | data formatting | bytes 524288 | tf_op args[3]
  7.9 2.0 %copy.25.vw_hbm = bf16[2048,64]{1,0:T(8,128)(2,1)} copy(bf16[2048,64]{0,1:T(8,128)(2,1)} %param.22) | data formatting | bytes 524288 | tf_op args[4]
  9.8 1.9 %copy.26.fw_hbm = bf16[2048,16]{1,0:T(8,128)(2,1)} copy(bf16[2048,16]{0,1:T(8,128)(2,1)} %param.23) | data formatting | bytes 131072 | tf_op args[5]
  11.7 48.4 %shard_map.201 = (bf16[16,2048]{1,0:T(8,128)(2,1)}, bf16[16,64]{1,0:T(8,128)(2,1)}, bf16[16,64]{1,0:T(8,128)(2,1)}, f32[16,16]{1,0:T(8,128)}) custom-call(s32[16]{0:T(128)} %len_ref.1, f32[16]{0:T(128)} %fbias_ref.1, bf16[16,2048]{1,0:T(8,128)(2,1)} %hid_ref.1, bf16[1,2048]{1,0:T(2,128)(2,1)} %broadcast_in_dim.6.again_ref, ...), custom_call_target="tpu_custom_call" | custom-call | tf_op jit(solution)/shard_map/pallas_call | solution.py:522
  60.2 1.5 %copy.31 = bf16[16,2048]{1,0:T(8,128)(2,1)} copy(bf16[16,2048]{1,0:T(8,128)(2,1)} %get-tuple-element.16) | data formatting | bytes 131072
  61.6 1.3 %copy.32 = bf16[16,1,64]{2,0,1:T(8,128)(2,1)} copy(bf16[16,1,64]{2,0,1:T(8,128)(2,1)} %bitcast.3) | data formatting | bytes 4096
  62.9 1.3 %copy.33 = bf16[16,1,64]{2,0,1:T(8,128)(2,1)} copy(bf16[16,1,64]{2,0,1:T(8,128)(2,1)} %bitcast.2) | data formatting | bytes 4096
  64.2 1.3 %copy.34 = f32[16,16]{1,0:T(8,128)} copy(f32[16,16]{1,0:T(8,128)} %get-tuple-element.19) | data formatting | bytes 2048

commit v2 on v1

--- a/solution.py
+++ b/solution.py
@@ -147,11 +147,11 @@
 PLANE = 4
 
 
-def step_body(n, len_ref, fbias_ref, hid_ref, again_ref, fgain_ref, ids_ref, rscore_ref,
+def step_body(n, len_hbm, fbias_hbm, hid_hbm, again_hbm, fgain_hbm, ids_hbm, rscore_hbm,
               qw_hbm, kw_hbm, vw_hbm, fw_hbm, keys_hbm, vals_hbm, logs_hbm, ow_hbm, gate_hbm, up_hbm, down_hbm,
               out_ref, key_ref, val_ref, nlog_ref,
-              qw, kw, vw, fw, keys, vals, logs, scores, maxes, lasts, sums, mixed_heads, att, ow, gate, up, down,
-              hidl, psend, pin, mixl, mixin, rows, ssq, wts, gacc, uacc, act, eout, back, fsum, far, upd,
+              len_ref, fbias_ref, hid_ref, again, fgain, fgain_row, ids_ref, rscore_ref, qw, kw, vw, fw, keys, vals, logs, scores, maxes, lasts, sums, mixed_heads, att, ow, gate, up, down,
+              hidl, psend, pin, mixl, mixin, rows, ssqz, ssqp, ssqt, wts, gacc, uacc, act, eout, back, fsum, far, upd,
               send, recv, local):
     f32, bf16 = jnp.float32, jnp.bfloat16
     me, tp = lax.axis_index("ep"), lax.axis_index("tp")
@@ -188,29 +188,32 @@
         used[kind] += count
         return base
 
-    sent = []
-
     def copy(src, dst, s, r, ep, core):
         return pltpu.make_async_remote_copy(src_ref=src, dst_ref=dst, send_sem=send.at[s], recv_sem=recv.at[r],
                                             device_id=(ep, core), device_id_type=MESH)
 
-    def begin(src, dst, r, ep, core):
-        c = copy(src, dst, take("s"), r, ep, core)
-        c.start()
-        sent.append(c)
-        return c
+    groups = []
+
+    def group(whole):
+        groups.append((take("s"), whole))
+        return groups[-1][0]
+
+    def begin(src, dst, s, r, ep, core):
+        copy(src, dst, s, r, ep, core).start()
 
     def arrived(dst, r):
         copy(dst, dst, 0, r, me, 1 - tp).wait_recv()
 
-    def load(src, dst):
-        c = pltpu.make_async_copy(src, dst, local.at[take("l")])
+    def load(src, dst, l=None):
+        c = pltpu.make_async_copy(src, dst, local.at[take("l") if l is None else l])
         c.start()
         return c
 
     def sl(i, size):
         return pl.ds(pl.multiple_of(i * size, size), size)
 
+    first = [load(hid_hbm, hid_ref), load(again_hbm, again), load(ids_hbm, ids_ref), load(rscore_hbm, rscore_ref)]
+    scalars = [load(fbias_hbm, fbias_ref), load(len_hbm, len_ref), load(fgain_hbm, fgain)]
     ow_load = load(ow_hbm.at[:, sl(tp, cols)], ow.at[xy])
     small = [load(kw_hbm, kw), load(vw_hbm, vw), load(fw_hbm, fw)]
     qchunk = width // 4
@@ -227,33 +230,43 @@
         pl.semaphore_signal(barrier, inc=1, device_id=(p, tp), device_id_type=MESH)
     pl.semaphore_signal(barrier, inc=1, device_id=(me, 1 - tp), device_id_type=MESH)
 
-    normed = root_norm(hid_ref[...], again_ref[...]).astype(bf16)
-    rscore = rscore_ref[...]
-    route = rscore / jnp.sum(rscore, axis=-1, keepdims=True)
-    lanes = lax.broadcasted_iota(jnp.int32, (seqs, 128), 1)
-    table = jnp.zeros((seqs, 128), f32)
-    for k in range(TOP_K):
-        table = table + jnp.where(lanes == ids_ref[:, k:k + 1], route[:, k:k + 1], 0.0)
-    wts[xy, sl(z, seqs), :] = table
-
     pl.semaphore_wait(barrier, outer - 1 + 3 + 1)
 
     hf = feats // 2
     lo, hi = pl.ds(0, hf), pl.ds(hf, hf)
     ow_load.wait()
-    ow_r = take("r", 6)
-    begin(ow.at[xy, lo], ow.at[xy, lo], ow_r, plane[0], tp)
-    begin(ow.at[xy, hi], ow.at[xy, hi], ow_r + 3, plane[1], tp)
-    begin(ow.at[xy, hi], ow.at[xy, hi], ow_r + 1, plane[0], tp)
-    begin(ow.at[xy, lo], ow.at[xy, lo], ow_r + 2, plane[1], tp)
-    hid_r = take("r", outer)
+    ow_s, ow_r = group(ow.at[pl.ds(0, 3)]), take("r", 3)
+    begin(ow.at[xy, lo], ow.at[xy, lo], ow_s, ow_r, plane[0], tp)
+    begin(ow.at[xy, hi], ow.at[xy, hi], ow_s, ow_r + 1, plane[1], tp)
+    begin(ow.at[xy, hi], ow.at[xy, hi], ow_s, ow_r + 2, plane[0], tp)
+    begin(ow.at[xy, lo], ow.at[xy, lo], ow_s, ow_r + 2, plane[1], tp)
+
+    for c in first:
+        c.wait()
+    normed = root_norm(hid_ref[...], again[...][None, :]).astype(bf16)
+    rscore = rscore_ref[...]
+    route = rscore / jnp.sum(rscore, axis=0, keepdims=True)
+    ids = ids_ref[...].astype(f32)
+    lanes = lax.broadcasted_iota(jnp.int32, (seqs, 128), 1).astype(f32)
+    small_eye = (lax.broadcasted_iota(jnp.int32, (seqs, seqs), 0) == lax.broadcasted_iota(jnp.int32, (seqs, seqs), 1))
+
+    def column(row):
+        return jnp.sum(jnp.where(small_eye, jnp.broadcast_to(row, (seqs, seqs)), 0.0), axis=1, keepdims=True)
+
+    table = jnp.zeros((seqs, 128), f32)
+    for k in range(TOP_K):
+        table = table + jnp.where(lanes == column(ids[k:k + 1, :]), column(route[k:k + 1, :]), 0.0)
+    wts[3, sl(z, seqs), :] = table
+
+    others = pl.ds(0, (outer - 1) * seqs)
+    hid_s, hid_r = group(hidl.at[others]), take("r")
     for zz in zs:
         begin(hid_ref.at[:, pl.ds(pl.multiple_of(zz * pf + tp * xq, xq), xq)], hidl.at[sl(z, seqs)],
-              hid_r + z, zdev(zz), tp)
+              hid_s, hid_r, zdev(zz), tp)
     hidl[sl(z, seqs), :] = hid_ref[:, pl.ds(pl.multiple_of(z * pf + tp * xq, xq), xq)]
-    wt_r = take("r", outer)
+    wt_s, wt_r = group(wts.at[0, others]), take("r")
     for zz in zs:
-        begin(wts.at[xy, sl(z, seqs)], wts.at[xy, sl(z, seqs)], wt_r + z, zdev(zz), tp)
+        begin(wts.at[3, sl(z, seqs)], wts.at[3, sl(z, seqs)], wt_s, wt_r, zdev(zz), tp)
 
     acc = jnp.zeros((seqs, cols), f32)
     for i in range(4):
@@ -263,29 +276,36 @@
     queries = acc.astype(bf16).astype(f32) * (HD ** -0.5)
     for c in small:
         c.wait()
-    key_new = jnp.dot(normed, kw[...], preferred_element_type=f32).astype(bf16)
-    value_new = jnp.dot(normed, vw[...], preferred_element_type=f32).astype(bf16)
+    for c in scalars:
+        c.wait()
+    fgain_row[...] = fgain[...].astype(f32)[None, :]
+
+    def new_token(w):
+        return lax.dot_general(normed, w[...], (((1,), (1,)), ((), ())), preferred_element_type=f32)
+
+    key_new = new_token(kw).astype(bf16)
+    value_new = new_token(vw).astype(bf16)
     key_ref[...] = key_new
     val_ref[...] = value_new
     hl = lax.broadcasted_iota(jnp.int32, (seqs, heads), 1)
     fb = jnp.zeros((seqs, heads), f32)
     for h in range(heads):
         fb = jnp.where(hl == h, fbias_ref[h], fb)
-    pre = jnp.dot(normed, fw[...], preferred_element_type=f32) + fb
+    pre = new_token(fw) + fb
     log_forget = jnp.minimum(pre, 0.0) - jnp.log1p(jnp.exp(-jnp.abs(pre)))
 
-    gate_loads, up_loads = [], []
+    gate_l, up_l, down_l = take("l"), take("l"), take("l")
     for t in range(2):
         for zc in range(outer):
             rows_from = pl.ds(zc * pf + t * xq, xq)
-            gate_loads.append(load(gate_hbm.at[0, rows_from], gate.at[t * outer + zc]))
-            up_loads.append(load(up_hbm.at[0, rows_from], up.at[t * outer + zc]))
-    down_loads, down_r = [], take("r", outer)
+            load(gate_hbm.at[0, rows_from], gate.at[t * outer + zc], gate_l)
+            load(up_hbm.at[0, rows_from], up.at[t * outer + zc], up_l)
+    down_s, down_r = group(down.at[0]), take("r")
     for zc in range(outer):
         mine = pl.ds(pl.multiple_of(zc * pf + tp * xq, xq), xq)
         other = pl.ds(pl.multiple_of(zc * pf + (1 - tp) * xq, xq), xq)
-        down_loads.append(load(down_hbm.at[0, :, mine], down.at[tp, :, pl.ds(zc * xq, xq)]))
-        begin(down_hbm.at[0, :, other], down.at[tp, :, pl.ds(zc * xq, xq)], down_r + zc, me, 1 - tp)
+        load(down_hbm.at[0, :, mine], down.at[tp, :, pl.ds(zc * xq, xq)], down_l)
+        begin(down_hbm.at[0, :, other], down.at[tp, :, pl.ds(zc * xq, xq)], down_s, down_r, me, 1 - tp)
 
     total = seqs * heads
 
@@ -342,27 +362,22 @@
         odd = mixed_heads[pl.ds(2 * j + 1, seqs, stride=heads), :]
         att[sl(z, seqs), j * 128:(j + 1) * 128] = jnp.where(wide < HD, even, odd).astype(bf16)
 
-    att_r = take("r", outer)
+    att_s, att_r = group(att.at[others]), take("r")
     for zz in reversed(zs):
-        begin(att.at[sl(z, seqs)], att.at[sl(z, seqs)], att_r + z, zdev(zz), tp)
+        begin(att.at[sl(z, seqs)], att.at[sl(z, seqs)], att_s, att_r, zdev(zz), tp)
     arrived(ow.at[spots[0], lo], ow_r)
-    relay_r = take("r", 2)
-    begin(ow.at[spots[0], lo], ow.at[spots[0], lo], relay_r, plane[1], tp)
-    arrived(ow.at[spots[1], hi], ow_r + 3)
-    begin(ow.at[spots[1], hi], ow.at[spots[1], hi], relay_r + 1, plane[0], tp)
-    for zz in zs:
-        arrived(wts.at[xy, sl(zz, seqs)], wt_r + zz)
-    wline_r = take("r", 3)
+    relay_r = take("r")
+    begin(ow.at[spots[0], lo], ow.at[spots[0], lo], ow_s, relay_r, plane[1], tp)
+    arrived(ow.at[spots[1], hi], ow_r + 1)
+    begin(ow.at[spots[1], hi], ow.at[spots[1], hi], ow_s, relay_r, plane[0], tp)
+    arrived(wts.at[0, others], wt_r)
+    wline_s, wline_r = group(wts.at[pl.ds(0, 3)]), take("r")
     for i in range(3):
-        begin(wts.at[xy], wts.at[xy], wline_r + i, plane[i], tp)
-    arrived(ow.at[spots[0], hi], ow_r + 1)
-    arrived(ow.at[spots[1], lo], ow_r + 2)
-    for zz in zs:
-        arrived(hidl.at[sl(zz, seqs)], hid_r + zz)
-    for zz in zs:
-        arrived(att.at[sl(zz, seqs)], att_r + zz)
-    arrived(ow.at[spots[2], lo], relay_r)
-    arrived(ow.at[spots[2], hi], relay_r + 1)
+        begin(wts.at[3], wts.at[i], wline_s, wline_r, plane[i], tp)
+    arrived(ow.at[0], ow_r + 2)
+    arrived(hidl.at[others], hid_r)
+    arrived(att.at[others], att_r)
+    arrived(ow.at[spots[2]], relay_r)
     lines = att[...]
 
     def project(t):
@@ -371,55 +386,61 @@
 
     for i, v in enumerate(project(1 - tp)):
         psend[:, i * feats:(i + 1) * feats] = v
-    p_r = take("r")
-    begin(psend, pin, p_r, me, 1 - tp)
+    p_s, p_r = group(psend), take("r")
+    begin(psend, pin, p_s, p_r, me, 1 - tp)
     kept = jnp.concatenate(project(tp), axis=1)
     arrived(pin, p_r)
     mixed = (kept + pin[...]).astype(bf16)
     residual = hidl[...].astype(f32) + mixed.astype(f32)
-    gain = fgain_ref[:, pl.ds(pl.multiple_of(z * pf + tp * xq, xq), xq)].astype(f32)
+    gain = fgain_row[:, pl.ds(pl.multiple_of(z * pf + tp * xq, xq), xq)]
     block = tp * outer + z
-    rows[block, xy] = (residual * gain).astype(bf16)
+    rows[block, 3] = (residual * gain).astype(bf16)
     square = jnp.sum(residual * residual, axis=-1, keepdims=True)
     eye = (lax.broadcasted_iota(jnp.int32, (line, line), 0) == lax.broadcasted_iota(jnp.int32, (line, line), 1))
     flat = jnp.sum(jnp.where(eye, jnp.broadcast_to(square, (line, line)), 0.0), axis=0, keepdims=True)
-    ssq[block, xy] = jnp.broadcast_to(flat, (8, line))
+    ssqz[z] = jnp.broadcast_to(flat, (8, line))
     mixl[...] = mixed
 
-    zrow_r, zsq_r = take("r", outer), take("r", outer)
-    prow_r, psq_r = take("r", 3 * outer), take("r", 3 * outer)
-    crow_r, csq_r = take("r", 4 * outer), take("r", 4 * outer)
+    zrow_s, zrow_r = group(rows.at[0, pl.ds(0, outer - 1)]), take("r", outer)
+    prow_s, prow_r = group(rows.at[pl.ds(0, 3)]), take("r", outer)
+    crow_s, crow_r = group(rows.at[pl.ds(0, outer)]), take("r", outer)
+    zsq_s, zsq_r = group(ssqz.at[pl.ds(0, outer - 1)]), take("r")
+    psq_s, psq_r = group(ssqt.at[pl.ds(0, 3)]), take("r")
+    csq_s, csq_r = group(ssqp.at[0]), take("r")
+    mix_s, mix_r = group(mixl.at[others]), take("r")
 
     def out_to_plane(zz):
         b = tp * outer + zz
-        for i in range(3):
-            begin(rows.at[b, xy], rows.at[b, xy], prow_r + i * outer + zz, plane[i], tp)
-            begin(ssq.at[b, xy], ssq.at[b, xy], psq_r + i * outer + zz, plane[i], tp)
-
-    def to_partner(zz, i, spot):
+        for i in (2, 0, 1):
+            begin(rows.at[b, 3], rows.at[b, i], prow_s, prow_r + zz, plane[i], tp)
+
+    def own_to_partner(zz):
         b = tp * outer + zz
-        begin(rows.at[b, spot], rows.at[b, spot], crow_r + i * outer + zz, me, 1 - tp)
-        begin(ssq.at[b, spot], ssq.at[b, spot], csq_r + i * outer + zz, me, 1 - tp)
+        begin(rows.at[b, 3], rows.at[b, 3], crow_s, crow_r + zz, me, 1 - tp)
 
     for zz in reversed(zs):
-        begin(rows.at[block, xy], rows.at[block, xy], zrow_r + z, zdev(zz), tp)
-        begin(ssq.at[block, xy], ssq.at[block, xy], zsq_r + z, zdev(zz), tp)
+        begin(rows.at[block, 3], rows.at[block, 3], zrow_s, zrow_r + z, zdev(zz), tp)
     out_to_plane(z)
-    to_partner(z, 3, xy)
-    mix_r = take("r", outer)
+    own_to_partner(z)
     for zz in zs:
-        begin(mixl.at[sl(zz, seqs)], mixin.at[z], mix_r + z, zdev(zz), tp)
+        begin(ssqz.at[z], ssqz.at[z], zsq_s, zsq_r, zdev(zz), tp)
     mixin[z] = mixl[sl(z, seqs), :]
     for zz in zs:
-        b = tp * outer + zz
-        arrived(rows.at[b, xy], zrow_r + zz)
-        arrived(ssq.at[b, xy], zsq_r + zz)
+        arrived(rows.at[tp * outer + zz, 3], zrow_r + zz)
         out_to_plane(zz)
-        to_partner(zz, 3, xy)
-    for c in gate_loads + up_loads + down_loads:
-        c.wait()
-    for i in range(3):
-        arrived(wts.at[spots[i]], wline_r + i)
+        own_to_partner(zz)
+    arrived(ssqz.at[pl.ds(0, outer - 1)], zsq_r)
+    squares = ssqz[0]
+    for i in range(1, outer):
+        squares = squares + ssqz[i]
+    ssqp[tp] = squares
+    begin(ssqp.at[tp], ssqp.at[tp], csq_s, csq_r, me, 1 - tp)
+    for zz in zs:
+        begin(mixl.at[sl(zz, seqs)], mixin.at[z], mix_s, mix_r, zdev(zz), tp)
+    pltpu.make_async_copy(gate, gate, local.at[gate_l]).wait()
+    pltpu.make_async_copy(up, up, local.at[up_l]).wait()
+    pltpu.make_async_copy(down.at[0], down.at[0], local.at[down_l]).wait()
+    arrived(wts.at[pl.ds(0, 3)], wline_r)
 
     def gather_block(t, zz, first):
         b = t * outer + zz
@@ -433,33 +454,32 @@
     for k in range(outer + 1):
         if k < outer:
             b = tp * outer + order[k]
+            theirs = rows.at[b, pl.ds(0, 3)]
+            arrived(theirs, prow_r + order[k])
+            begin(theirs, theirs, crow_s, crow_r + order[k], me, 1 - tp)
+            gather_block(tp, order[k], k == 0)
+        if k == 0:
+            arrived(ssqp.at[1 - tp], csq_r)
+            ssqt[3] = ssqp[0] + ssqp[1]
             for i in range(3):
-                arrived(rows.at[b, spots[i]], prow_r + i * outer + order[k])
-                arrived(ssq.at[b, spots[i]], psq_r + i * outer + order[k])
-                to_partner(order[k], i, spots[i])
-            gather_block(tp, order[k], k == 0)
+                begin(ssqt.at[3], ssqt.at[i], psq_s, psq_r, plane[i], tp)
         if k > 0:
             b = (1 - tp) * outer + order[k - 1]
-            for i, spot in enumerate(spots + [xy]):
-                arrived(rows.at[b, spot], crow_r + i * outer + order[k - 1])
-                arrived(ssq.at[b, spot], csq_r + i * outer + order[k - 1])
+            arrived(rows.at[b], crow_r + order[k - 1])
             gather_block(1 - tp, order[k - 1], False)
+    arrived(ssqt.at[pl.ds(0, 3)], psq_r)
     for q in range(PLANE):
-        whole = ssq[0, q][:1, :]
-        for b in range(1, 2 * outer):
-            whole = whole + ssq[b, q][:1, :]
-        scale = lax.rsqrt(whole * (1.0 / width) + epsilon)
+        scale = lax.rsqrt(ssqt[q][:1, :] * (1.0 / width) + epsilon)
         scale = jnp.sum(jnp.where(eye, jnp.broadcast_to(scale, (line, line)), 0.0), axis=1, keepdims=True)
         g = gacc[pl.ds(q * line, line), :] * scale
         u = uacc[pl.ds(q * line, line), :] * scale
         act[tp, q] = (g / (1.0 + jnp.exp(-g)) * u).astype(bf16)
-    act_r = take("r")
-    begin(act.at[tp], act.at[tp], act_r, me, 1 - tp)
-    for zc in range(outer):
-        arrived(down.at[1 - tp, :, pl.ds(zc * xq, xq)], down_r + zc)
+    act_s, act_r = group(act.at[0]), take("r")
+    begin(act.at[tp], act.at[tp], act_s, act_r, me, 1 - tp)
+    arrived(down.at[1 - tp], down_r)
     arrived(act.at[1 - tp], act_r)
 
-    back_r = take("r", 3 * outer)
+    back_s, back_r = group(eout.at[pl.ds(0, 3)]), take("r", outer)
     out_order = list(reversed(zs)) + [z]
     which = lax.broadcasted_iota(jnp.int32, (PLANE * seqs, 128), 1) == me
     for zz in out_order:
@@ -471,33 +491,32 @@
                 + jnp.dot(tokens(act.at[1]), down[1], preferred_element_type=f32)) * weight
         eout[zz] = made.astype(bf16).reshape(PLANE, seqs, made.shape[1])
         for i in (2, 0, 1):
-            begin(eout.at[zz, spots[i]], back.at[i, zz], back_r + i * outer + zz, plane[i], tp)
-    far_r = take("r", outer)
+            begin(eout.at[zz, i], back.at[zz, i], back_s, back_r + zz, plane[i], tp)
+    far_s, far_r = group(fsum.at[pl.ds(0, outer - 1)]), take("r")
     for zz in out_order:
-        summed = eout[zz, xy].astype(f32)
+        summed = eout[zz, 3].astype(f32)
+        arrived(back.at[zz], back_r + zz)
         for i in range(3):
-            arrived(back.at[i, zz], back_r + i * outer + zz)
-            summed = summed + back[i, zz].astype(f32)
+            summed = summed + back[zz, i].astype(f32)
         if zz is not z:
             fsum[zz] = summed.astype(bf16)
-            begin(fsum.at[zz], far.at[z], far_r + z, zdev(zz), tp)
+            begin(fsum.at[zz], far.at[z], far_s, far_r, zdev(zz), tp)
+    arrived(mixin.at[pl.ds(0, outer - 1)], mix_r)
+    arrived(far.at[pl.ds(0, outer - 1)], far_r)
     for zz in zs:
-        arrived(mixin.at[zz], mix_r + zz)
-    for zz in zs:
-        arrived(far.at[zz], far_r + zz)
         summed = summed + far[zz].astype(f32)
     for zc in range(outer):
         here = hid_ref[:, pl.ds(pl.multiple_of(zc * pf + tp * xq, xq), xq)].astype(f32) + mixin[zc].astype(f32)
         upd[tp, :, zc * xq:(zc + 1) * xq] = (here + summed[:, zc * xq:(zc + 1) * xq]).astype(bf16)
-    u_r = take("r")
-    begin(upd.at[tp], upd.at[tp], u_r, me, 1 - tp)
+    u_s, u_r = group(upd.at[0]), take("r")
+    begin(upd.at[tp], upd.at[tp], u_s, u_r, me, 1 - tp)
     arrived(upd.at[1 - tp], u_r)
     for t in range(2):
         for zc in range(outer):
             out_ref[:, zc * pf + t * xq:zc * pf + (t + 1) * xq] = upd[t, :, zc * xq:(zc + 1) * xq]
-    for c in sent:
-        c.wait_send()
-    assert used["s"] <= send.shape[0] and used["r"] <= recv.shape[0] and used["l"] <= local.shape[0], used
+    for s, whole in groups:
+        copy(whole, whole, s, 0, me, 1 - tp).wait_send()
+    assert used["s"] == send.shape[0] and used["r"] == recv.shape[0] and used["l"] == local.shape[0], used
 
 
 def step_kernel(hidden, attn_gain, query_weight, key_weight, value_weight, forget_weight, forget_bias,
@@ -516,17 +535,17 @@
     half = width // 2
     bf16, f32 = jnp.bfloat16, jnp.float32
     vmem = pl.BlockSpec(memory_space=pltpu.VMEM)
-    smem = pl.BlockSpec(memory_space=pltpu.SMEM)
-    hbm = pl.BlockSpec(memory_space=pl.ANY)
+    hbm = pl.BlockSpec(memory_space=pltpu.HBM)
     v = pltpu.VMEM
-    updated, key_new, value_new, new_logsum = pl.pallas_call(
+    results = pl.pallas_call(
         functools.partial(step_body, n),
-        out_shape=[jax.ShapeDtypeStruct((seqs, width), bf16), jax.ShapeDtypeStruct((seqs, HD), bf16),
-                   jax.ShapeDtypeStruct((seqs, HD), bf16), jax.ShapeDtypeStruct((seqs, heads), f32)],
-        in_specs=[smem] * 2 + [vmem] * 5 + [hbm] * 11,
+        out_shape=[v((seqs, width), bf16), v((seqs, HD), bf16), v((seqs, HD), bf16), v((seqs, heads), f32)],
+        in_specs=[hbm] * 18,
         out_specs=[vmem] * 4,
         scratch_shapes=[
-            v((width, cols), bf16), v((width, HD), bf16), v((width, HD), bf16), v((width, heads), bf16),
+            pltpu.SMEM((seqs,), jnp.int32), pltpu.SMEM((heads,), f32), v((seqs, width), bf16), v((width,), bf16),
+            v((width,), bf16), v((1, width), f32), v((TOP_K, seqs), jnp.int32), v((TOP_K, seqs), f32),
+            v((width, cols), bf16), v((HD, width), bf16), v((HD, width), bf16), v((heads, width), bf16),
             v((seqs, HD, cache_len), bf16), v((seqs, HD, cache_len), bf16), v((seqs, heads, cache_len), f32),
             v((seqs * heads, cache_len), f32), v((seqs * heads, 128), f32), v((seqs * heads, 128), f32),
             v((seqs * heads, 128), f32), v((seqs * heads, 2 * HD), f32),
@@ -534,17 +553,30 @@
             v((2 * outer, xq, units), bf16), v((2 * outer, xq, units), bf16), v((2, units, half), bf16),
             v((line, xq), bf16), v((line, xq), f32), v((line, xq), f32), v((line, xq), bf16),
             v((outer, seqs, xq), bf16),
-            v((2 * outer, PLANE, line, xq), bf16), v((2 * outer, PLANE, 8, line), f32), v((PLANE, line, 128), f32),
+            v((2 * outer, PLANE, line, xq), bf16), v((outer, 8, line), f32), v((2, 8, line), f32),
+            v((PLANE, 8, line), f32), v((PLANE, line, 128), f32),
             v((PLANE * line, units), f32), v((PLANE * line, units), f32), v((2, PLANE, line, units), bf16),
-            v((outer, PLANE, seqs, half), bf16), v((3, outer, seqs, half), bf16),
+            v((outer, PLANE, seqs, half), bf16), v((outer, 3, seqs, half), bf16),
             v((outer, seqs, half), bf16), v((outer, seqs, half), bf16), v((2, seqs, half), bf16),
-            pltpu.SemaphoreType.DMA((200,)), pltpu.SemaphoreType.DMA((200,)), pltpu.SemaphoreType.DMA((64,)),
+            pltpu.SemaphoreType.DMA((18,)), pltpu.SemaphoreType.DMA((17 + 4 * outer,)), pltpu.SemaphoreType.DMA((30,)),
         ],
         compiler_params=pltpu.CompilerParams(
-            collective_id=0, has_side_effects=True, vmem_limit_bytes=60 * 1024 * 1024),
-    )(lengths, forget_bias, hidden, attn_gain[None, :], ffn_gain[None, :], expert_ids, expert_scores,
-      query_weight, key_weight, value_weight, forget_weight, cache_keys, cache_values, cache_logsum,
-      out_weight, gate_weights, up_weights, down_weights)
+            collective_id=0, has_side_effects=True, vmem_limit_bytes=40 * 1024 * 1024),
+    )(*[pltpu.with_memory_space_constraint(a, pltpu.HBM) for a in (
+        lengths, forget_bias, hidden, attn_gain, ffn_gain, expert_ids.T, expert_scores.T,
+        query_weight, key_weight.T, value_weight.T, forget_weight.T, cache_keys, cache_values, cache_logsum,
+        out_weight, gate_weights, up_weights, down_weights)])
+
+    def hand_out(*refs):
+        for i in range(4):
+            refs[4 + i][...] = refs[i][...]
+
+    updated, key_new, value_new, new_logsum = pl.pallas_call(
+        hand_out,
+        out_shape=[jax.ShapeDtypeStruct(r.shape, r.dtype) for r in results],
+        in_specs=[vmem] * 4,
+        out_specs=[vmem] * 4,
+    )(*[pltpu.with_memory_space_constraint(r, pltpu.VMEM) for r in results])
     return updated, key_new.reshape(seqs, 1, HD), value_new.reshape(seqs, 1, HD), new_logsum
 
 

time: 66 us -> 43.7 us (0.66)
  local copies, waits for them, and re-layouts: 16.4 us -> 0 us
  Pallas kernels: 48.4 us -> 42.9 us
    unnamed x9 -> x0, local copies, waits for them, and re-layouts: 13.8 us -> none
    pallas_call x1 -> x2, Pallas kernels: 48.4 us -> 42.9 us  [the longest x1 42.3 us: step_kernel(): pl.pallas_call(functools.partial(step_body, n), out_shape=[v((seqs, width...]
    broadcast_in_dim x2 -> x0, local copies, waits for them, and re-layouts: 2.58 us -> none  [the longest x1 1.29 us: step_kernel(): attn_gain[None, :]]
where the time goes in v2:
time: 43.7 us; the launch traced here: 43.6 us
  Pallas kernels  42.9 us (98%)
  between operations  0.65 us (1%)
    pallas_call x1, Pallas kernels, step_kernel(): pl.pallas_call(functools.partial(step_body, n), out_shape=[v((seqs, width...  42.3 us

profile of v2, /device:TPU:0, one launch (start us, length us, event | category | flops | bytes accessed | tf_op | source)
XLA Modules:
  0.0 43.6 jit_solution(10512306765487751536)
XLA Ops:
  0.6 42.3 %shard_map.201 = (bf16[16,2048]{1,0:T(8,128)(2,1)S(1)}, bf16[16,64]{1,0:T(8,128)(2,1)S(1)}, bf16[16,64]{1,0:T(8,128)(2,1)S(1)}, f32[16,16]{1,0:T(8,128)S(1)}) custom-call(s32[16]{0:T(128)} %len_hbm.1, f32[16]{0:T(128)} %fbias_hbm.1, bf16[16,2048]{1,0:T(8,128)(2,1)} %hid_hbm.1, bf16[2048]{0:T(1024)(128)(2,1)} %again_hbm.1, bf16[2048]{0:T(1024)(128)(2,1)} %fgain_hbm.1, ...), custom_call_target="tpu_custom_call" | custom-call | tf_op jit(solution)/shard_map/pallas_call | solution.py:540
  42.9 0.6 %shard_map.202 = (bf16[16,2048]{1,0:T(8,128)(2,1)}, bf16[16,64]{1,0:T(8,128)(2,1)}, bf16[16,64]{1,0:T(8,128)(2,1)}, f32[16,16]{1,0:T(8,128)}) custom-call(bf16[16,2048]{1,0:T(8,128)(2,1)S(1)} %get-tuple-element.12.refs_0_, bf16[16,64]{1,0:T(8,128)(2,1)S(1)} %get-tuple-element.13.refs_1_, bf16[16,64]{1,0:T(8,128)(2,1)S(1)} %get-tuple-element.14.refs_2_, ...), custom_call_target="tpu_custom_call" | custom-call | tf_op jit(solution)/shard_map/pallas_call | solution.py:574

commit v3 on v2

--- a/solution.py
+++ b/solution.py
@@ -151,7 +151,7 @@
               qw_hbm, kw_hbm, vw_hbm, fw_hbm, keys_hbm, vals_hbm, logs_hbm, ow_hbm, gate_hbm, up_hbm, down_hbm,
               out_ref, key_ref, val_ref, nlog_ref,
               len_ref, fbias_ref, hid_ref, again, fgain, fgain_row, ids_ref, rscore_ref, qw, kw, vw, fw, keys, vals, logs, scores, maxes, lasts, sums, mixed_heads, att, ow, gate, up, down,
-              hidl, psend, pin, mixl, mixin, rows, ssqz, ssqp, ssqt, wts, gacc, uacc, act, eout, back, fsum, far, upd,
+              hidl, part, pin, mixl, mixin, rows, ssq, ssqp, scales, wts, act, eout, back, fsum, far, upd,
               send, recv, local):
     f32, bf16 = jnp.float32, jnp.bfloat16
     me, tp = lax.axis_index("ep"), lax.axis_index("tp")
@@ -173,14 +173,20 @@
         return zz * PLANE + xy
 
     near_tables = [sorted([j for j in range(outer) if j != i], key=lambda j: (abs(j - i), j)) for i in range(outer)]
-
-    def nth(k):
-        value = near_tables[0][k]
+    far_tables = [sorted(range(outer), key=lambda j: (-abs(j - i), j)) for i in range(outer)]
+
+    def pick(tables, k, zz):
+        value = tables[0][k]
         for i in range(1, outer):
-            value = jnp.where(z == i, near_tables[i][k], value)
+            value = jnp.where(zz == i, tables[i][k], value)
         return value
 
-    zs = [nth(k) for k in range(outer - 1)]
+    zs = [pick(near_tables, k, z) for k in range(outer - 1)]
+    dests = [pick(far_tables, k, z) for k in range(outer - 1)] + [z]
+
+    def rows_of(g, zz):
+        return sl(zz if g == outer - 1 else pick(far_tables, g, zz), seqs)
+
     used = {"s": 0, "r": 0, "l": 0}
 
     def take(kind, count=1):
@@ -192,11 +198,13 @@
         return pltpu.make_async_remote_copy(src_ref=src, dst_ref=dst, send_sem=send.at[s], recv_sem=recv.at[r],
                                             device_id=(ep, core), device_id_type=MESH)
 
-    groups = []
+    wholes = [0, 0]
 
     def group(whole):
-        groups.append((take("s"), whole))
-        return groups[-1][0]
+        size = math.prod(whole.shape) * whole.dtype.itemsize
+        kind = 0 if size % (32 * cols) == 0 else 1
+        wholes[kind] += size
+        return kind
 
     def begin(src, dst, s, r, ep, core):
         copy(src, dst, s, r, ep, core).start()
@@ -211,17 +219,6 @@
 
     def sl(i, size):
         return pl.ds(pl.multiple_of(i * size, size), size)
-
-    first = [load(hid_hbm, hid_ref), load(again_hbm, again), load(ids_hbm, ids_ref), load(rscore_hbm, rscore_ref)]
-    scalars = [load(fbias_hbm, fbias_ref), load(len_hbm, len_ref), load(fgain_hbm, fgain)]
-    ow_load = load(ow_hbm.at[:, sl(tp, cols)], ow.at[xy])
-    small = [load(kw_hbm, kw), load(vw_hbm, vw), load(fw_hbm, fw)]
-    qchunk = width // 4
-    qw_loads = [load(qw_hbm.at[pl.ds(i * qchunk, qchunk)], qw.at[pl.ds(i * qchunk, qchunk)]) for i in range(4)]
-    part = seqs // 4
-    key_loads = [load(keys_hbm.at[pl.ds(i * part, part), 0], keys.at[pl.ds(i * part, part)]) for i in range(4)]
-    log_loads = [load(logs_hbm.at[pl.ds(i * part, part)], logs.at[pl.ds(i * part, part)]) for i in range(4)]
-    val_loads = [load(vals_hbm.at[pl.ds(i * part, part), 0], vals.at[pl.ds(i * part, part)]) for i in range(4)]
 
     barrier = pltpu.get_barrier_semaphore()
     for d in range(1, outer):
@@ -229,6 +226,17 @@
     for p in plane:
         pl.semaphore_signal(barrier, inc=1, device_id=(p, tp), device_id_type=MESH)
     pl.semaphore_signal(barrier, inc=1, device_id=(me, 1 - tp), device_id_type=MESH)
+
+    ow_load = load(ow_hbm.at[:, sl(tp, cols)], ow.at[xy])
+    first = [load(hid_hbm, hid_ref), load(again_hbm, again), load(ids_hbm, ids_ref), load(rscore_hbm, rscore_ref)]
+    scalars = [load(fbias_hbm, fbias_ref), load(len_hbm, len_ref), load(fgain_hbm, fgain)]
+    small = [load(kw_hbm, kw), load(vw_hbm, vw), load(fw_hbm, fw)]
+    qchunk = width // 4
+    qw_loads = [load(qw_hbm.at[pl.ds(i * qchunk, qchunk)], qw.at[pl.ds(i * qchunk, qchunk)]) for i in range(4)]
+    batch = seqs // 2
+    key_loads = [load(keys_hbm.at[pl.ds(i * batch, batch), 0], keys.at[pl.ds(i * batch, batch)]) for i in range(2)]
+    log_loads = [load(logs_hbm.at[pl.ds(i * batch, batch)], logs.at[pl.ds(i * batch, batch)]) for i in range(2)]
+    val_loads = [load(vals_hbm.at[pl.ds(i * batch, batch), 0], vals.at[pl.ds(i * batch, batch)]) for i in range(2)]
 
     pl.semaphore_wait(barrier, outer - 1 + 3 + 1)
 
@@ -322,9 +330,9 @@
 
     positions = lax.broadcasted_iota(jnp.int32, (heads, cache_len), 1)
     for s in range(seqs):
-        if s % part == 0:
-            key_loads[s // part].wait()
-            log_loads[s // part].wait()
+        if s % batch == 0:
+            key_loads[s // batch].wait()
+            log_loads[s // batch].wait()
         here = pl.ds(s * heads, heads)
         size = len_ref[s]
         level = logs[s]
@@ -344,8 +352,8 @@
     peak = jnp.maximum(maxes[:, :1], own)
     maxes[...] = jnp.broadcast_to(peak, (total, 128))
     for s in range(seqs):
-        if s % part == 0:
-            val_loads[s // part].wait()
+        if s % batch == 0:
+            val_loads[s // batch].wait()
         here = pl.ds(s * heads, heads)
         weights = jnp.exp(scores[here, :] - maxes[here, :][:, :1])
         sums[here, :] = jnp.broadcast_to(jnp.sum(weights, axis=-1, keepdims=True), (heads, 128))
@@ -377,20 +385,19 @@
     arrived(ow.at[0], ow_r + 2)
     arrived(hidl.at[others], hid_r)
     arrived(att.at[others], att_r)
+    lines = att[...]
+
+    def project(i):
+        part[i] = lax.dot_general(lines, ow[i], (((1,), (1,)), ((), ())), preferred_element_type=f32)
+
+    for i in [xy] + spots[:2]:
+        project(i)
     arrived(ow.at[spots[2]], relay_r)
-    lines = att[...]
-
-    def project(t):
-        return [lax.dot_general(lines, ow[2 * t + i], (((1,), (1,)), ((), ())), preferred_element_type=f32)
-                for i in range(2)]
-
-    for i, v in enumerate(project(1 - tp)):
-        psend[:, i * feats:(i + 1) * feats] = v
-    p_s, p_r = group(psend), take("r")
-    begin(psend, pin, p_s, p_r, me, 1 - tp)
-    kept = jnp.concatenate(project(tp), axis=1)
+    project(spots[2])
+    p_s, p_r = group(pin), take("r")
+    begin(part.at[pl.ds(2 * (1 - tp), 2)], pin, p_s, p_r, me, 1 - tp)
     arrived(pin, p_r)
-    mixed = (kept + pin[...]).astype(bf16)
+    mixed = jnp.concatenate([part[2 * tp + i] + pin[i] for i in range(2)], axis=1).astype(bf16)
     residual = hidl[...].astype(f32) + mixed.astype(f32)
     gain = fgain_row[:, pl.ds(pl.multiple_of(z * pf + tp * xq, xq), xq)]
     block = tp * outer + z
@@ -398,43 +405,39 @@
     square = jnp.sum(residual * residual, axis=-1, keepdims=True)
     eye = (lax.broadcasted_iota(jnp.int32, (line, line), 0) == lax.broadcasted_iota(jnp.int32, (line, line), 1))
     flat = jnp.sum(jnp.where(eye, jnp.broadcast_to(square, (line, line)), 0.0), axis=0, keepdims=True)
-    ssqz[z] = jnp.broadcast_to(flat, (8, line))
+    ssq[z, 3] = jnp.broadcast_to(flat, (8, line))
     mixl[...] = mixed
 
-    zrow_s, zrow_r = group(rows.at[0, pl.ds(0, outer - 1)]), take("r", outer)
+    zrow_s, zrow_r = group(rows.at[0, pl.ds(0, outer - 1)]), take("r", outer * outer)
     prow_s, prow_r = group(rows.at[pl.ds(0, 3)]), take("r", outer)
     crow_s, crow_r = group(rows.at[pl.ds(0, outer)]), take("r", outer)
-    zsq_s, zsq_r = group(ssqz.at[pl.ds(0, outer - 1)]), take("r")
-    psq_s, psq_r = group(ssqt.at[pl.ds(0, 3)]), take("r")
-    csq_s, csq_r = group(ssqp.at[0]), take("r")
+    zsq_s, zsq_r = 2, take("r")
+    psq_s, psq_r = 3, take("r")
+    csq_s, csq_r = 3, take("r")
     mix_s, mix_r = group(mixl.at[others]), take("r")
 
-    def out_to_plane(zz):
-        b = tp * outer + zz
+    def out_to_plane(g, zz):
+        b, some = tp * outer + zz, rows_of(g, z)
         for i in (2, 0, 1):
-            begin(rows.at[b, 3], rows.at[b, i], prow_s, prow_r + zz, plane[i], tp)
-
-    def own_to_partner(zz):
-        b = tp * outer + zz
-        begin(rows.at[b, 3], rows.at[b, 3], crow_s, crow_r + zz, me, 1 - tp)
-
-    for zz in reversed(zs):
-        begin(rows.at[block, 3], rows.at[block, 3], zrow_s, zrow_r + z, zdev(zz), tp)
-    out_to_plane(z)
-    own_to_partner(z)
-    for zz in zs:
-        begin(ssqz.at[z], ssqz.at[z], zsq_s, zsq_r, zdev(zz), tp)
+            begin(rows.at[b, 3, some], rows.at[b, i, some], prow_s, prow_r + g, plane[i], tp)
+
+    for g in range(outer):
+        for zz in reversed(zs):
+            some = rows_of(g, zz)
+            begin(rows.at[block, 3, some], rows.at[block, 3, some], zrow_s, zrow_r + g * outer + z, zdev(zz), tp)
+        if g == 0:
+            for zz in reversed(zs):
+                begin(ssq.at[z, 3], ssq.at[z, 3], zsq_s, zsq_r, zdev(zz), tp)
+        out_to_plane(g, z)
     mixin[z] = mixl[sl(z, seqs), :]
-    for zz in zs:
-        arrived(rows.at[tp * outer + zz, 3], zrow_r + zz)
-        out_to_plane(zz)
-        own_to_partner(zz)
-    arrived(ssqz.at[pl.ds(0, outer - 1)], zsq_r)
-    squares = ssqz[0]
-    for i in range(1, outer):
-        squares = squares + ssqz[i]
-    ssqp[tp] = squares
-    begin(ssqp.at[tp], ssqp.at[tp], csq_s, csq_r, me, 1 - tp)
+    for g in range(outer):
+        for zz in zs:
+            arrived(rows.at[tp * outer + zz, 3, rows_of(g, z)], zrow_r + g * outer + zz)
+            out_to_plane(g, zz)
+        if g == 0:
+            arrived(ssq.at[0, pl.ds(0, outer - 1)], zsq_r)
+            for i in range(3):
+                begin(ssq.at[:, 3], ssq.at[:, i], psq_s, psq_r, plane[i], tp)
     for zz in zs:
         begin(mixl.at[sl(zz, seqs)], mixin.at[z], mix_s, mix_r, zdev(zz), tp)
     pltpu.make_async_copy(gate, gate, local.at[gate_l]).wait()
@@ -442,58 +445,88 @@
     pltpu.make_async_copy(down.at[0], down.at[0], local.at[down_l]).wait()
     arrived(wts.at[pl.ds(0, 3)], wline_r)
 
-    def gather_block(t, zz, first):
-        b = t * outer + zz
-        left = rows[b].reshape(PLANE * line, xq)
-        g = jnp.dot(left, gate[b], preferred_element_type=f32)
-        u = jnp.dot(left, up[b], preferred_element_type=f32)
-        gacc[...] = g if first else gacc[...] + g
-        uacc[...] = u if first else uacc[...] + u
-
-    order = [z] + zs
-    for k in range(outer + 1):
-        if k < outer:
-            b = tp * outer + order[k]
-            theirs = rows.at[b, pl.ds(0, 3)]
-            arrived(theirs, prow_r + order[k])
-            begin(theirs, theirs, crow_s, crow_r + order[k], me, 1 - tp)
-            gather_block(tp, order[k], k == 0)
-        if k == 0:
-            arrived(ssqp.at[1 - tp], csq_r)
-            ssqt[3] = ssqp[0] + ssqp[1]
-            for i in range(3):
-                begin(ssqt.at[3], ssqt.at[i], psq_s, psq_r, plane[i], tp)
-        if k > 0:
-            b = (1 - tp) * outer + order[k - 1]
-            arrived(rows.at[b], crow_r + order[k - 1])
-            gather_block(1 - tp, order[k - 1], False)
-    arrived(ssqt.at[pl.ds(0, 3)], psq_r)
+    parts = [[g] for g in range(outer // 2)] + [list(range(outer // 2, outer))]
+
+    def product(part_groups, t):
+        left = jnp.concatenate([
+            jnp.concatenate([rows[t * outer + i, :, rows_of(g, z), :].reshape(PLANE * seqs, xq) for g in part_groups],
+                            axis=0) for i in range(outer)], axis=1)
+        span = pl.ds(t * outer, outer)
+        return [jnp.dot(left, w[span].reshape(outer * xq, w.shape[2]), preferred_element_type=f32) for w in (gate, up)]
+
+    def pass_on(part_groups):
+        for g in part_groups:
+            span, some = pl.ds(tp * outer, outer), rows_of(g, z)
+            arrived(rows.at[span, pl.ds(0, 3), some], prow_r + g)
+            block_rows = rows.at[span, :, some]
+            begin(block_rows, block_rows, crow_s, crow_r + g, me, 1 - tp)
+
+    def collect(part_groups, early):
+        for g in part_groups:
+            arrived(rows.at[pl.ds((1 - tp) * outer, outer), :, rows_of(g, z)], crow_r + g)
+        late = product(part_groups, 1 - tp)
+        return early[0] + late[0], early[1] + late[1]
+
+    act_s, act_r = group(act.at[0]), take("r", outer)
+
+    def span_of(part_groups):
+        return pl.ds(part_groups[0], len(part_groups))
+
+    def activate(part_groups, a, u):
+        scale = jnp.concatenate([scales[:, rows_of(g, z), :].reshape(PLANE * seqs, 128)[:, :1] for g in part_groups],
+                                axis=0)
+        a, u = a * scale, u * scale
+        made = (a / (1.0 + jnp.exp(-a)) * u).astype(bf16)
+        here = act.at[tp, span_of(part_groups)]
+        here[...] = made.reshape(len(part_groups), PLANE * seqs, made.shape[1])
+        begin(here, here, act_s, act_r + part_groups[0], me, 1 - tp)
+
+    back_s, back_r = group(eout.at[pl.ds(0, 3)]), take("r", outer)
+    which = lax.broadcasted_iota(jnp.int32, (PLANE * seqs, 128), 1) == me
+
+    def give(part_groups):
+        span = span_of(part_groups)
+        arrived(act.at[1 - tp, span], act_r + part_groups[0])
+        lefts = [act[t, span].reshape(len(part_groups) * PLANE * seqs, act.shape[3]) for t in range(2)]
+        made = (jnp.dot(lefts[0], down[0], preferred_element_type=f32)
+                + jnp.dot(lefts[1], down[1], preferred_element_type=f32))
+        for j, g in enumerate(part_groups):
+            zz = dests[g]
+            wt = wts[:, sl(zz, seqs), :].reshape(PLANE * seqs, 128)
+            weight = jnp.sum(jnp.where(which, wt, 0.0), axis=-1, keepdims=True)
+            scaled = made[j * PLANE * seqs:(j + 1) * PLANE * seqs] * weight
+            eout[zz] = scaled.astype(bf16).reshape(PLANE, seqs, made.shape[1])
+            for i in (2, 0, 1):
+                begin(eout.at[zz, i], back.at[zz, i], back_s, back_r + zz, plane[i], tp)
+
+    arrived(ssq.at[:, pl.ds(0, 3)], psq_r)
+    squares = ssq[0]
+    for i in range(1, outer):
+        squares = squares + ssq[i]
+    ssqp[tp] = squares
+    begin(ssqp.at[tp], ssqp.at[tp], csq_s, csq_r, me, 1 - tp)
+    pass_on(parts[0])
+    early = product(parts[0], tp)
+    pass_on(parts[1])
+    a, u = collect(parts[0], early)
+    arrived(ssqp.at[1 - tp], csq_r)
+    squares = ssqp[0] + ssqp[1]
     for q in range(PLANE):
-        scale = lax.rsqrt(ssqt[q][:1, :] * (1.0 / width) + epsilon)
+        scale = lax.rsqrt(squares[q, :1, :] * (1.0 / width) + epsilon)
         scale = jnp.sum(jnp.where(eye, jnp.broadcast_to(scale, (line, line)), 0.0), axis=1, keepdims=True)
-        g = gacc[pl.ds(q * line, line), :] * scale
-        u = uacc[pl.ds(q * line, line), :] * scale
-        act[tp, q] = (g / (1.0 + jnp.exp(-g)) * u).astype(bf16)
-    act_s, act_r = group(act.at[0]), take("r")
-    begin(act.at[tp], act.at[tp], act_s, act_r, me, 1 - tp)
+        scales[q] = jnp.broadcast_to(scale, (line, 128))
+    activate(parts[0], a, u)
     arrived(down.at[1 - tp], down_r)
-    arrived(act.at[1 - tp], act_r)
-
-    back_s, back_r = group(eout.at[pl.ds(0, 3)]), take("r", outer)
-    out_order = list(reversed(zs)) + [z]
-    which = lax.broadcasted_iota(jnp.int32, (PLANE * seqs, 128), 1) == me
-    for zz in out_order:
-        def tokens(ref):
-            return ref[:, sl(zz, seqs), :].reshape(PLANE * seqs, ref.shape[2])
-
-        weight = jnp.sum(jnp.where(which, tokens(wts), 0.0), axis=-1, keepdims=True)
-        made = (jnp.dot(tokens(act.at[0]), down[0], preferred_element_type=f32)
-                + jnp.dot(tokens(act.at[1]), down[1], preferred_element_type=f32)) * weight
-        eout[zz] = made.astype(bf16).reshape(PLANE, seqs, made.shape[1])
-        for i in (2, 0, 1):
-            begin(eout.at[zz, i], back.at[zz, i], back_s, back_r + zz, plane[i], tp)
+    for k in range(1, len(parts)):
+        early = product(parts[k], tp)
+        if k + 1 < len(parts):
+            pass_on(parts[k + 1])
+        a, u = collect(parts[k], early)
+        activate(parts[k], a, u)
+        give(parts[k - 1])
+    give(parts[-1])
     far_s, far_r = group(fsum.at[pl.ds(0, outer - 1)]), take("r")
-    for zz in out_order:
+    for zz in dests:
         summed = eout[zz, 3].astype(f32)
         arrived(back.at[zz], back_r + zz)
         for i in range(3):
@@ -514,9 +547,11 @@
     for t in range(2):
         for zc in range(outer):
             out_ref[:, zc * pf + t * xq:zc * pf + (t + 1) * xq] = upd[t, :, zc * xq:(zc + 1) * xq]
-    for s, whole in groups:
+    assert wholes[0] % (32 * cols) == 0 and wholes[1] % 4096 == 0, wholes
+    for s, whole in enumerate((qw.at[pl.ds(0, wholes[0] // (2 * cols))], maxes.at[pl.ds(0, wholes[1] // 512)],
+                               ssq.at[0, pl.ds(0, outer - 1)], ssq)):
         copy(whole, whole, s, 0, me, 1 - tp).wait_send()
-    assert used["s"] == send.shape[0] and used["r"] == recv.shape[0] and used["l"] == local.shape[0], used
+    assert used["r"] == recv.shape[0] and used["l"] == local.shape[0], used
 
 
 def step_kernel(hidden, attn_gain, query_weight, key_weight, value_weight, forget_weight, forget_bias,
@@ -551,14 +586,14 @@
             v((seqs * heads, 128), f32), v((seqs * heads, 2 * HD), f32),
             v((line, cols), bf16), v((PLANE, feats, cols), bf16),
             v((2 * outer, xq, units), bf16), v((2 * outer, xq, units), bf16), v((2, units, half), bf16),
-            v((line, xq), bf16), v((line, xq), f32), v((line, xq), f32), v((line, xq), bf16),
+            v((line, xq), bf16), v((PLANE, line, feats), f32), v((2, line, feats), f32), v((line, xq), bf16),
             v((outer, seqs, xq), bf16),
-            v((2 * outer, PLANE, line, xq), bf16), v((outer, 8, line), f32), v((2, 8, line), f32),
-            v((PLANE, 8, line), f32), v((PLANE, line, 128), f32),
-            v((PLANE * line, units), f32), v((PLANE * line, units), f32), v((2, PLANE, line, units), bf16),
+            v((2 * outer, PLANE, line, xq), bf16), v((outer, PLANE, 8, line), f32), v((2, PLANE, 8, line), f32),
+            v((PLANE, line, 128), f32), v((PLANE, line, 128), f32),
+                        v((2, outer, PLANE * seqs, units), bf16),
             v((outer, PLANE, seqs, half), bf16), v((outer, 3, seqs, half), bf16),
             v((outer, seqs, half), bf16), v((outer, seqs, half), bf16), v((2, seqs, half), bf16),
-            pltpu.SemaphoreType.DMA((18,)), pltpu.SemaphoreType.DMA((17 + 4 * outer,)), pltpu.SemaphoreType.DMA((30,)),
+            pltpu.SemaphoreType.DMA((4,)), pltpu.SemaphoreType.DMA((16 + 4 * outer + outer * outer,)), pltpu.SemaphoreType.DMA((24,)),
         ],
         compiler_params=pltpu.CompilerParams(
             collective_id=0, has_side_effects=True, vmem_limit_bytes=40 * 1024 * 1024),
@@ -586,7 +621,7 @@
     n = lax.axis_size("ep")
     seqs, width = hidden.shape
     fits = (
-        n % PLANE == 0
+        n % (2 * PLANE) == 0
         and lax.axis_size("tp") == 2
         and gate_weights.shape[0] == 1
         and cache_keys.shape[1] == 1

time: 43.7 us -> 39.7 us (0.908)
  Pallas kernels: 42.9 us -> 38.9 us
    pallas_call x1, Pallas kernels: 42.3 us -> 38.2 us  [step_kernel(): pl.pallas_call(functools.partial(step_body, n), out_shape=[v((seqs, width...]
where the time goes in v3:
time: 39.7 us; the launch traced here: 39.5 us
  Pallas kernels  38.9 us (98%)
  between operations  0.65 us (2%)
    pallas_call x1, Pallas kernels, step_kernel(): pl.pallas_call(functools.partial(step_body, n), out_shape=[v((seqs, width...  38.2 us

profile of v3, /device:TPU:0, one launch (start us, length us, event | category | flops | bytes accessed | tf_op | source)
XLA Modules:
  0.0 39.5 jit_solution(15978657685428396991)
XLA Ops:
  0.6 38.2 %shard_map.201 = (bf16[16,2048]{1,0:T(8,128)(2,1)S(1)}, bf16[16,64]{1,0:T(8,128)(2,1)S(1)}, bf16[16,64]{1,0:T(8,128)(2,1)S(1)}, f32[16,16]{1,0:T(8,128)S(1)}) custom-call(s32[16]{0:T(128)} %len_hbm.1, f32[16]{0:T(128)} %fbias_hbm.1, bf16[16,2048]{1,0:T(8,128)(2,1)} %hid_hbm.1, bf16[2048]{0:T(1024)(128)(2,1)} %again_hbm.1, bf16[2048]{0:T(1024)(128)(2,1)} %fgain_hbm.1, ...), custom_call_target="tpu_custom_call" | custom-call | tf_op jit(solution)/shard_map/pallas_call | solution.py:575
  38.9 0.6 %shard_map.202 = (bf16[16,2048]{1,0:T(8,128)(2,1)}, bf16[16,64]{1,0:T(8,128)(2,1)}, bf16[16,64]{1,0:T(8,128)(2,1)}, f32[16,16]{1,0:T(8,128)}) custom-call(bf16[16,2048]{1,0:T(8,128)(2,1)S(1)} %get-tuple-element.12.refs_0_, bf16[16,64]{1,0:T(8,128)(2,1)S(1)} %get-tuple-element.13.refs_1_, bf16[16,64]{1,0:T(8,128)(2,1)S(1)} %get-tuple-element.14.refs_2_, ...), custom_call_target="tpu_custom_call" | custom-call | tf_op jit(solution)/shard_map/pallas_call | solution.py:609

commit v4 on v3

--- a/solution.py
+++ b/solution.py
@@ -150,8 +150,8 @@
 def step_body(n, len_hbm, fbias_hbm, hid_hbm, again_hbm, fgain_hbm, ids_hbm, rscore_hbm,
               qw_hbm, kw_hbm, vw_hbm, fw_hbm, keys_hbm, vals_hbm, logs_hbm, ow_hbm, gate_hbm, up_hbm, down_hbm,
               out_ref, key_ref, val_ref, nlog_ref,
-              len_ref, fbias_ref, hid_ref, again, fgain, fgain_row, ids_ref, rscore_ref, qw, kw, vw, fw, keys, vals, logs, scores, maxes, lasts, sums, mixed_heads, att, ow, gate, up, down,
-              hidl, part, pin, mixl, mixin, rows, ssq, ssqp, scales, wts, act, eout, back, fsum, far, upd,
+              len_ref, fbias_ref, hid_ref, again, fgain, fgain_row, ids_ref, rscore_ref, qw, kw, vw, fw, keys, vals, logs, scores, maxes, lasts, sums, mixed_heads, att, wsend, ow, gate, up, down,
+              hidl, part, mixl, mixin, rows, ssq, ssqp, scales, wts, act, eout, back, fsum, far, upd,
               send, recv, local):
     f32, bf16 = jnp.float32, jnp.bfloat16
     me, tp = lax.axis_index("ep"), lax.axis_index("tp")
@@ -160,7 +160,7 @@
     heads = cols // HD
     cache_len = keys.shape[2]
     outer = n // PLANE
-    feats = ow.shape[1]
+    feats = wsend.shape[0]
     pf = PLANE * feats
     xq = pf // 2
     line = outer * seqs
@@ -225,29 +225,45 @@
         pl.semaphore_signal(barrier, inc=1, device_id=(zdev(lax.rem(z + d, outer)), tp), device_id_type=MESH)
     for p in plane:
         pl.semaphore_signal(barrier, inc=1, device_id=(p, tp), device_id_type=MESH)
+    for p in plane[:2]:
+        pl.semaphore_signal(barrier, inc=1, device_id=(p, 1 - tp), device_id_type=MESH)
     pl.semaphore_signal(barrier, inc=1, device_id=(me, 1 - tp), device_id_type=MESH)
 
-    ow_load = load(ow_hbm.at[:, sl(tp, cols)], ow.at[xy])
+    ow_load = load(ow_hbm.at[:, sl(tp, cols)], wsend)
+    first_core, slot, own_l = xy // 2, lax.rem(xy, 2), take("l")
+
+    @pl.when(tp == first_core)
+    def own_rows():
+        load(ow_hbm, ow.at[slot], own_l)
+
     first = [load(hid_hbm, hid_ref), load(again_hbm, again), load(ids_hbm, ids_ref), load(rscore_hbm, rscore_ref)]
     scalars = [load(fbias_hbm, fbias_ref), load(len_hbm, len_ref), load(fgain_hbm, fgain)]
-    small = [load(kw_hbm, kw), load(vw_hbm, vw), load(fw_hbm, fw)]
+    small_l, qw_l, keys_l, logs_l, vals_l = [take("l") for _ in range(5)]
+    for src, dst in ((kw_hbm, kw), (vw_hbm, vw), (fw_hbm, fw)):
+        load(src, dst, small_l)
     qchunk = width // 4
-    qw_loads = [load(qw_hbm.at[pl.ds(i * qchunk, qchunk)], qw.at[pl.ds(i * qchunk, qchunk)]) for i in range(4)]
-    batch = seqs // 2
-    key_loads = [load(keys_hbm.at[pl.ds(i * batch, batch), 0], keys.at[pl.ds(i * batch, batch)]) for i in range(2)]
-    log_loads = [load(logs_hbm.at[pl.ds(i * batch, batch)], logs.at[pl.ds(i * batch, batch)]) for i in range(2)]
-    val_loads = [load(vals_hbm.at[pl.ds(i * batch, batch), 0], vals.at[pl.ds(i * batch, batch)]) for i in range(2)]
-
-    pl.semaphore_wait(barrier, outer - 1 + 3 + 1)
+    for i in range(4):
+        load(qw_hbm.at[pl.ds(i * qchunk, qchunk)], qw.at[pl.ds(i * qchunk, qchunk)], qw_l)
+    batch = seqs // 4
+    for i in range(4):
+        some = pl.ds(i * batch, batch)
+        load(keys_hbm.at[some, 0], keys.at[some], keys_l)
+        load(logs_hbm.at[some], logs.at[some], logs_l)
+    for i in range(4):
+        some = pl.ds(i * batch, batch)
+        load(vals_hbm.at[some, 0], vals.at[some], vals_l)
+
+    def loaded(ref, l):
+        pltpu.make_async_copy(ref, ref, local.at[l]).wait()
+
+    pl.semaphore_wait(barrier, outer - 1 + 3 + 2 + 1)
 
     hf = feats // 2
     lo, hi = pl.ds(0, hf), pl.ds(hf, hf)
     ow_load.wait()
-    ow_s, ow_r = group(ow.at[pl.ds(0, 3)]), take("r", 3)
-    begin(ow.at[xy, lo], ow.at[xy, lo], ow_s, ow_r, plane[0], tp)
-    begin(ow.at[xy, hi], ow.at[xy, hi], ow_s, ow_r + 1, plane[1], tp)
-    begin(ow.at[xy, hi], ow.at[xy, hi], ow_s, ow_r + 2, plane[0], tp)
-    begin(ow.at[xy, lo], ow.at[xy, lo], ow_s, ow_r + 2, plane[1], tp)
+    ow_s, ow_r = group(ow.at[0]), take("r", 3)
+    for i, some, r in ((0, lo, 0), (1, hi, 1), (0, hi, 2), (1, lo, 2)):
+        begin(wsend.at[some], ow.at[slot, some, sl(tp, cols)], ow_s, ow_r + r, plane[i], first_core)
 
     for c in first:
         c.wait()
@@ -276,14 +292,10 @@
     for zz in zs:
         begin(wts.at[3, sl(z, seqs)], wts.at[3, sl(z, seqs)], wt_s, wt_r, zdev(zz), tp)
 
-    acc = jnp.zeros((seqs, cols), f32)
-    for i in range(4):
-        qw_loads[i].wait()
-        acc = acc + jnp.dot(normed[:, i * qchunk:(i + 1) * qchunk], qw[pl.ds(i * qchunk, qchunk), :],
-                            preferred_element_type=f32)
+    loaded(qw, qw_l)
+    acc = jnp.dot(normed, qw[...], preferred_element_type=f32)
     queries = acc.astype(bf16).astype(f32) * (HD ** -0.5)
-    for c in small:
-        c.wait()
+    loaded(qw.at[pl.ds(0, (2 * HD + heads) * width // cols)], small_l)
     for c in scalars:
         c.wait()
     fgain_row[...] = fgain[...].astype(f32)[None, :]
@@ -302,17 +314,17 @@
     pre = new_token(fw) + fb
     log_forget = jnp.minimum(pre, 0.0) - jnp.log1p(jnp.exp(-jnp.abs(pre)))
 
-    gate_l, up_l, down_l = take("l"), take("l"), take("l")
+    expert_l = take("l")
     for t in range(2):
         for zc in range(outer):
             rows_from = pl.ds(zc * pf + t * xq, xq)
-            load(gate_hbm.at[0, rows_from], gate.at[t * outer + zc], gate_l)
-            load(up_hbm.at[0, rows_from], up.at[t * outer + zc], up_l)
+            load(gate_hbm.at[0, rows_from], gate.at[t * outer + zc], expert_l)
+            load(up_hbm.at[0, rows_from], up.at[t * outer + zc], expert_l)
     down_s, down_r = group(down.at[0]), take("r")
     for zc in range(outer):
         mine = pl.ds(pl.multiple_of(zc * pf + tp * xq, xq), xq)
         other = pl.ds(pl.multiple_of(zc * pf + (1 - tp) * xq, xq), xq)
-        load(down_hbm.at[0, :, mine], down.at[tp, :, pl.ds(zc * xq, xq)], down_l)
+        load(down_hbm.at[0, :, mine], down.at[tp, :, pl.ds(zc * xq, xq)], expert_l)
         begin(down_hbm.at[0, :, other], down.at[tp, :, pl.ds(zc * xq, xq)], down_s, down_r, me, 1 - tp)
 
     total = seqs * heads
@@ -330,9 +342,9 @@
 
     positions = lax.broadcasted_iota(jnp.int32, (heads, cache_len), 1)
     for s in range(seqs):
-        if s % batch == 0:
-            key_loads[s // batch].wait()
-            log_loads[s // batch].wait()
+        if s == 0:
+            loaded(keys, keys_l)
+            loaded(logs, logs_l)
         here = pl.ds(s * heads, heads)
         size = len_ref[s]
         level = logs[s]
@@ -352,8 +364,8 @@
     peak = jnp.maximum(maxes[:, :1], own)
     maxes[...] = jnp.broadcast_to(peak, (total, 128))
     for s in range(seqs):
-        if s % batch == 0:
-            val_loads[s // batch].wait()
+        if s == 0:
+            loaded(vals, vals_l)
         here = pl.ds(s * heads, heads)
         weights = jnp.exp(scores[here, :] - maxes[here, :][:, :1])
         sums[here, :] = jnp.broadcast_to(jnp.sum(weights, axis=-1, keepdims=True), (heads, 128))
@@ -368,36 +380,53 @@
     for j in range(cols // 128):
         even = mixed_heads[pl.ds(2 * j, seqs, stride=heads), :]
         odd = mixed_heads[pl.ds(2 * j + 1, seqs, stride=heads), :]
-        att[sl(z, seqs), j * 128:(j + 1) * 128] = jnp.where(wide < HD, even, odd).astype(bf16)
-
-    att_s, att_r = group(att.at[others]), take("r")
+        att[tp, sl(z, seqs), j * 128:(j + 1) * 128] = jnp.where(wide < HD, even, odd).astype(bf16)
+
+    att_s, att_r = group(att.at[0, others]), take("r")
     for zz in reversed(zs):
-        begin(att.at[sl(z, seqs)], att.at[sl(z, seqs)], att_s, att_r, zdev(zz), tp)
-    arrived(ow.at[spots[0], lo], ow_r)
-    relay_r = take("r")
-    begin(ow.at[spots[0], lo], ow.at[spots[0], lo], ow_s, relay_r, plane[1], tp)
-    arrived(ow.at[spots[1], hi], ow_r + 1)
-    begin(ow.at[spots[1], hi], ow.at[spots[1], hi], ow_s, relay_r, plane[0], tp)
+        begin(att.at[tp, sl(z, seqs)], att.at[tp, sl(z, seqs)], att_s, att_r, zdev(zz), tp)
+    relay_s, relay_r = group(ow.at[0, lo]), take("r")
+
+    @pl.when(tp == first_core)
+    def relay_along_y():
+        half = ow.at[1 - slot, lo]
+        arrived(half, ow_r)
+        begin(half, half, relay_s, relay_r, plane[1], tp)
+
+    @pl.when(tp != first_core)
+    def relay_along_x():
+        half = ow.at[slot, hi]
+        arrived(half, ow_r + 1)
+        begin(half, half, relay_s, relay_r, plane[0], tp)
+
     arrived(wts.at[0, others], wt_r)
     wline_s, wline_r = group(wts.at[pl.ds(0, 3)]), take("r")
     for i in range(3):
         begin(wts.at[3], wts.at[i], wline_s, wline_r, plane[i], tp)
-    arrived(ow.at[0], ow_r + 2)
     arrived(hidl.at[others], hid_r)
-    arrived(att.at[others], att_r)
-    lines = att[...]
+    arrived(att.at[0, others], att_r)
+    both_s, both_r = group(att.at[0]), take("r")
+    begin(att.at[tp], att.at[tp], both_s, both_r, me, 1 - tp)
+    arrived(ow.at[0, lo], ow_r + 2)
+
+    @pl.when(tp == first_core)
+    def own_rows_there():
+        loaded(ow.at[slot], own_l)
+
+    arrived(att.at[1 - tp], both_r)
+    lines = jnp.concatenate([att[0], att[1]], axis=1)
 
     def project(i):
         part[i] = lax.dot_general(lines, ow[i], (((1,), (1,)), ((), ())), preferred_element_type=f32)
 
-    for i in [xy] + spots[:2]:
-        project(i)
-    arrived(ow.at[spots[2]], relay_r)
-    project(spots[2])
-    p_s, p_r = group(pin), take("r")
-    begin(part.at[pl.ds(2 * (1 - tp), 2)], pin, p_s, p_r, me, 1 - tp)
-    arrived(pin, p_r)
-    mixed = jnp.concatenate([part[2 * tp + i] + pin[i] for i in range(2)], axis=1).astype(bf16)
+    project(slot)
+
+    @pl.when(tp != first_core)
+    def last_rows_there():
+        arrived(ow.at[1 - slot], relay_r)
+
+    project(1 - slot)
+    mixed = jnp.concatenate([part[0], part[1]], axis=1).astype(bf16)
     residual = hidl[...].astype(f32) + mixed.astype(f32)
     gain = fgain_row[:, pl.ds(pl.multiple_of(z * pf + tp * xq, xq), xq)]
     block = tp * outer + z
@@ -408,7 +437,7 @@
     ssq[z, 3] = jnp.broadcast_to(flat, (8, line))
     mixl[...] = mixed
 
-    zrow_s, zrow_r = group(rows.at[0, pl.ds(0, outer - 1)]), take("r", outer * outer)
+    zrow_s, zrow_r = group(rows.at[0, pl.ds(0, outer - 1)]), take("r", 2 * outer - 1)
     prow_s, prow_r = group(rows.at[pl.ds(0, 3)]), take("r", outer)
     crow_s, crow_r = group(rows.at[pl.ds(0, outer)]), take("r", outer)
     zsq_s, zsq_r = 2, take("r")
@@ -424,15 +453,18 @@
     for g in range(outer):
         for zz in reversed(zs):
             some = rows_of(g, zz)
-            begin(rows.at[block, 3, some], rows.at[block, 3, some], zrow_s, zrow_r + g * outer + z, zdev(zz), tp)
+            begin(rows.at[block, 3, some], rows.at[block, 3, some], zrow_s, zrow_r + (z if g == 0 else outer - 1 + g), zdev(zz), tp)
         if g == 0:
             for zz in reversed(zs):
                 begin(ssq.at[z, 3], ssq.at[z, 3], zsq_s, zsq_r, zdev(zz), tp)
         out_to_plane(g, z)
     mixin[z] = mixl[sl(z, seqs), :]
     for g in range(outer):
+        if g:
+            arrived(rows.at[pl.ds(0, outer - 1), 3, rows_of(g, z)], zrow_r + outer - 1 + g)
         for zz in zs:
-            arrived(rows.at[tp * outer + zz, 3, rows_of(g, z)], zrow_r + g * outer + zz)
+            if g == 0:
+                arrived(rows.at[tp * outer + zz, 3, rows_of(g, z)], zrow_r + zz)
             out_to_plane(g, zz)
         if g == 0:
             arrived(ssq.at[0, pl.ds(0, outer - 1)], zsq_r)
@@ -440,12 +472,11 @@
                 begin(ssq.at[:, 3], ssq.at[:, i], psq_s, psq_r, plane[i], tp)
     for zz in zs:
         begin(mixl.at[sl(zz, seqs)], mixin.at[z], mix_s, mix_r, zdev(zz), tp)
-    pltpu.make_async_copy(gate, gate, local.at[gate_l]).wait()
-    pltpu.make_async_copy(up, up, local.at[up_l]).wait()
-    pltpu.make_async_copy(down.at[0], down.at[0], local.at[down_l]).wait()
+    units = gate.shape[2]
+    loaded(qw.at[pl.ds(0, (2 * width * units + units * width // 2) // cols)], expert_l)
     arrived(wts.at[pl.ds(0, 3)], wline_r)
 
-    parts = [[g] for g in range(outer // 2)] + [list(range(outer // 2, outer))]
+    parts = [[g] for g in range(outer)]
 
     def product(part_groups, t):
         left = jnp.concatenate([
@@ -517,23 +548,36 @@
         scales[q] = jnp.broadcast_to(scale, (line, 128))
     activate(parts[0], a, u)
     arrived(down.at[1 - tp], down_r)
+    far_s, far_r = group(fsum.at[pl.ds(0, outer - 1)]), take("r")
+
+    def near(g):
+        zz = dests[g]
+        arrived(back.at[zz], back_r + zz)
+        summed = eout[zz, 3].astype(f32)
+        for i in range(3):
+            summed = summed + back[zz, i].astype(f32)
+        if g < outer - 1:
+            fsum[zz] = summed.astype(bf16)
+            begin(fsum.at[zz], far.at[z], far_s, far_r, zdev(zz), tp)
+        return summed
+
+    last = len(parts) - 1
     for k in range(1, len(parts)):
         early = product(parts[k], tp)
-        if k + 1 < len(parts):
+        if k == last:
+            give(parts[k - 1])
+        elif k > 1:
             pass_on(parts[k + 1])
         a, u = collect(parts[k], early)
         activate(parts[k], a, u)
-        give(parts[k - 1])
-    give(parts[-1])
-    far_s, far_r = group(fsum.at[pl.ds(0, outer - 1)]), take("r")
-    for zz in dests:
-        summed = eout[zz, 3].astype(f32)
-        arrived(back.at[zz], back_r + zz)
-        for i in range(3):
-            summed = summed + back[zz, i].astype(f32)
-        if zz is not z:
-            fsum[zz] = summed.astype(bf16)
-            begin(fsum.at[zz], far.at[z], far_s, far_r, zdev(zz), tp)
+        if k == 1:
+            pass_on(parts[2])
+        if k < last:
+            give(parts[k - 1])
+    near(0)
+    give(parts[last])
+    for g in range(1, outer):
+        summed = near(g)
     arrived(mixin.at[pl.ds(0, outer - 1)], mix_r)
     arrived(far.at[pl.ds(0, outer - 1)], far_r)
     for zz in zs:
@@ -584,16 +628,16 @@
             v((seqs, HD, cache_len), bf16), v((seqs, HD, cache_len), bf16), v((seqs, heads, cache_len), f32),
             v((seqs * heads, cache_len), f32), v((seqs * heads, 128), f32), v((seqs * heads, 128), f32),
             v((seqs * heads, 128), f32), v((seqs * heads, 2 * HD), f32),
-            v((line, cols), bf16), v((PLANE, feats, cols), bf16),
+            v((2, line, cols), bf16), v((feats, cols), bf16), v((2, feats, 2 * cols), bf16),
             v((2 * outer, xq, units), bf16), v((2 * outer, xq, units), bf16), v((2, units, half), bf16),
-            v((line, xq), bf16), v((PLANE, line, feats), f32), v((2, line, feats), f32), v((line, xq), bf16),
+            v((line, xq), bf16), v((2, line, feats), f32), v((line, xq), bf16),
             v((outer, seqs, xq), bf16),
             v((2 * outer, PLANE, line, xq), bf16), v((outer, PLANE, 8, line), f32), v((2, PLANE, 8, line), f32),
             v((PLANE, line, 128), f32), v((PLANE, line, 128), f32),
                         v((2, outer, PLANE * seqs, units), bf16),
             v((outer, PLANE, seqs, half), bf16), v((outer, 3, seqs, half), bf16),
             v((outer, seqs, half), bf16), v((outer, seqs, half), bf16), v((2, seqs, half), bf16),
-            pltpu.SemaphoreType.DMA((4,)), pltpu.SemaphoreType.DMA((16 + 4 * outer + outer * outer,)), pltpu.SemaphoreType.DMA((24,)),
+            pltpu.SemaphoreType.DMA((4,)), pltpu.SemaphoreType.DMA((15 + 6 * outer,)), pltpu.SemaphoreType.DMA((15,)),
         ],
         compiler_params=pltpu.CompilerParams(
             collective_id=0, has_side_effects=True, vmem_limit_bytes=40 * 1024 * 1024),
@@ -628,6 +672,7 @@
         and seqs % 16 == 0
         and (query_weight.shape[1] // HD) % 16 == 0
         and out_weight.shape[0] % 128 == 0
+        and n >= 4 * PLANE
         and n <= 128
     )
     if fits:

time: 39.7 us -> 38.1 us (0.960)
  Pallas kernels: 38.9 us -> 37.3 us
    pallas_call x1, Pallas kernels: 38.2 us -> 36.6 us  [step_kernel(): pl.pallas_call(functools.partial(step_body, n), out_shape=[v((seqs, width...]
where the time goes in v4:
time: 38.1 us; the launch traced here: 37.9 us
  Pallas kernels  37.3 us (98%)
  between operations  0.65 us (2%)
    pallas_call x1, Pallas kernels, step_kernel(): pl.pallas_call(functools.partial(step_body, n), out_shape=[v((seqs, width...  36.6 us

profile of v4, /device:TPU:0, one launch (start us, length us, event | category | flops | bytes accessed | tf_op | source)
XLA Modules:
  0.0 37.9 jit_solution(7465639449980619370)
XLA Ops:
  0.6 36.6 %shard_map.201 = (bf16[16,2048]{1,0:T(8,128)(2,1)S(1)}, bf16[16,64]{1,0:T(8,128)(2,1)S(1)}, bf16[16,64]{1,0:T(8,128)(2,1)S(1)}, f32[16,16]{1,0:T(8,128)S(1)}) custom-call(s32[16]{0:T(128)} %len_hbm.1, f32[16]{0:T(128)} %fbias_hbm.1, bf16[16,2048]{1,0:T(8,128)(2,1)} %hid_hbm.1, bf16[2048]{0:T(1024)(128)(2,1)} %again_hbm.1, bf16[2048]{0:T(1024)(128)(2,1)} %fgain_hbm.1, ...), custom_call_target="tpu_custom_call" | custom-call | tf_op jit(solution)/shard_map/pallas_call | solution.py:619
  37.3 0.6 %shard_map.202 = (bf16[16,2048]{1,0:T(8,128)(2,1)}, bf16[16,64]{1,0:T(8,128)(2,1)}, bf16[16,64]{1,0:T(8,128)(2,1)}, f32[16,16]{1,0:T(8,128)}) custom-call(bf16[16,2048]{1,0:T(8,128)(2,1)S(1)} %get-tuple-element.12.refs_0_, bf16[16,64]{1,0:T(8,128)(2,1)S(1)} %get-tuple-element.13.refs_1_, bf16[16,64]{1,0:T(8,128)(2,1)S(1)} %get-tuple-element.14.refs_2_, ...), custom_call_target="tpu_custom_call" | custom-call | tf_op jit(solution)/shard_map/pallas_call | solution.py:653

commit v5 on v4

--- a/solution.py
+++ b/solution.py
@@ -151,7 +151,7 @@
               qw_hbm, kw_hbm, vw_hbm, fw_hbm, keys_hbm, vals_hbm, logs_hbm, ow_hbm, gate_hbm, up_hbm, down_hbm,
               out_ref, key_ref, val_ref, nlog_ref,
               len_ref, fbias_ref, hid_ref, again, fgain, fgain_row, ids_ref, rscore_ref, qw, kw, vw, fw, keys, vals, logs, scores, maxes, lasts, sums, mixed_heads, att, wsend, ow, gate, up, down,
-              hidl, part, mixl, mixin, rows, ssq, ssqp, scales, wts, act, eout, back, fsum, far, upd,
+              hidl, part, mixl, mixin, rows, ssq, ssqp, scales, wts, begun, act, eout, back, fsum, far, upd,
               send, recv, local):
     f32, bf16 = jnp.float32, jnp.bfloat16
     me, tp = lax.axis_index("ep"), lax.axis_index("tp")
@@ -232,10 +232,6 @@
     ow_load = load(ow_hbm.at[:, sl(tp, cols)], wsend)
     first_core, slot, own_l = xy // 2, lax.rem(xy, 2), take("l")
 
-    @pl.when(tp == first_core)
-    def own_rows():
-        load(ow_hbm, ow.at[slot], own_l)
-
     first = [load(hid_hbm, hid_ref), load(again_hbm, again), load(ids_hbm, ids_ref), load(rscore_hbm, rscore_ref)]
     scalars = [load(fbias_hbm, fbias_ref), load(len_hbm, len_ref), load(fgain_hbm, fgain)]
     small_l, qw_l, keys_l, logs_l, vals_l = [take("l") for _ in range(5)]
@@ -261,9 +257,15 @@
     hf = feats // 2
     lo, hi = pl.ds(0, hf), pl.ds(hf, hf)
     ow_load.wait()
-    ow_s, ow_r = group(ow.at[0]), take("r", 3)
-    for i, some, r in ((0, lo, 0), (1, hi, 1), (0, hi, 2), (1, lo, 2)):
+    ow_s, ow_r = group(ow.at[0]), take("r", 5)
+    quarters = [pl.ds(k * hf // 2, hf // 2) for k in range(4)]
+    for i, some, r in ((0, quarters[0], 0), (1, quarters[2], 1), (0, quarters[1], 2), (1, quarters[3], 3),
+                       (0, hi, 4), (1, lo, 4)):
         begin(wsend.at[some], ow.at[slot, some, sl(tp, cols)], ow_s, ow_r + r, plane[i], first_core)
+
+    @pl.when(tp == first_core)
+    def own_rows():
+        load(ow_hbm, ow.at[slot], own_l)
 
     for c in first:
         c.wait()
@@ -389,15 +391,17 @@
 
     @pl.when(tp == first_core)
     def relay_along_y():
-        half = ow.at[1 - slot, lo]
-        arrived(half, ow_r)
-        begin(half, half, relay_s, relay_r, plane[1], tp)
+        for k in range(2):
+            piece = ow.at[1 - slot, quarters[k]]
+            arrived(piece, ow_r + 2 * k)
+            begin(piece, piece, relay_s, relay_r, plane[1], tp)
 
     @pl.when(tp != first_core)
     def relay_along_x():
-        half = ow.at[slot, hi]
-        arrived(half, ow_r + 1)
-        begin(half, half, relay_s, relay_r, plane[0], tp)
+        for k in range(2):
+            piece = ow.at[slot, quarters[2 + k]]
+            arrived(piece, ow_r + 1 + 2 * k)
+            begin(piece, piece, relay_s, relay_r, plane[0], tp)
 
     arrived(wts.at[0, others], wt_r)
     wline_s, wline_r = group(wts.at[pl.ds(0, 3)]), take("r")
@@ -407,7 +411,7 @@
     arrived(att.at[0, others], att_r)
     both_s, both_r = group(att.at[0]), take("r")
     begin(att.at[tp], att.at[tp], both_s, both_r, me, 1 - tp)
-    arrived(ow.at[0, lo], ow_r + 2)
+    arrived(ow.at[0, lo], ow_r + 4)
 
     @pl.when(tp == first_core)
     def own_rows_there():
@@ -492,11 +496,17 @@
             block_rows = rows.at[span, :, some]
             begin(block_rows, block_rows, crow_s, crow_r + g, me, 1 - tp)
 
-    def collect(part_groups, early):
+    def start(part_groups):
+        k = part_groups[0] % 2
+        for i, v in enumerate(product(part_groups, tp)):
+            begun[k, i] = v
+        return k
+
+    def collect(part_groups, k):
         for g in part_groups:
             arrived(rows.at[pl.ds((1 - tp) * outer, outer), :, rows_of(g, z)], crow_r + g)
         late = product(part_groups, 1 - tp)
-        return early[0] + late[0], early[1] + late[1]
+        return begun[k, 0] + late[0], begun[k, 1] + late[1]
 
     act_s, act_r = group(act.at[0]), take("r", outer)
 
@@ -530,14 +540,14 @@
             for i in (2, 0, 1):
                 begin(eout.at[zz, i], back.at[zz, i], back_s, back_r + zz, plane[i], tp)
 
+    pass_on(parts[0])
     arrived(ssq.at[:, pl.ds(0, 3)], psq_r)
     squares = ssq[0]
     for i in range(1, outer):
         squares = squares + ssq[i]
     ssqp[tp] = squares
     begin(ssqp.at[tp], ssqp.at[tp], csq_s, csq_r, me, 1 - tp)
-    pass_on(parts[0])
-    early = product(parts[0], tp)
+    early = start(parts[0])
     pass_on(parts[1])
     a, u = collect(parts[0], early)
     arrived(ssqp.at[1 - tp], csq_r)
@@ -563,7 +573,7 @@
 
     last = len(parts) - 1
     for k in range(1, len(parts)):
-        early = product(parts[k], tp)
+        early = start(parts[k])
         if k == last:
             give(parts[k - 1])
         elif k > 1:
@@ -634,10 +644,10 @@
             v((outer, seqs, xq), bf16),
             v((2 * outer, PLANE, line, xq), bf16), v((outer, PLANE, 8, line), f32), v((2, PLANE, 8, line), f32),
             v((PLANE, line, 128), f32), v((PLANE, line, 128), f32),
-                        v((2, outer, PLANE * seqs, units), bf16),
+                        v((2, 2, PLANE * seqs, units), f32), v((2, outer, PLANE * seqs, units), bf16),
             v((outer, PLANE, seqs, half), bf16), v((outer, 3, seqs, half), bf16),
             v((outer, seqs, half), bf16), v((outer, seqs, half), bf16), v((2, seqs, half), bf16),
-            pltpu.SemaphoreType.DMA((4,)), pltpu.SemaphoreType.DMA((15 + 6 * outer,)), pltpu.SemaphoreType.DMA((15,)),
+            pltpu.SemaphoreType.DMA((4,)), pltpu.SemaphoreType.DMA((17 + 6 * outer,)), pltpu.SemaphoreType.DMA((15,)),
         ],
         compiler_params=pltpu.CompilerParams(
             collective_id=0, has_side_effects=True, vmem_limit_bytes=40 * 1024 * 1024),

time: 38.1 us -> 37.5 us (0.984)
  Pallas kernels: 37.3 us -> 36.7 us
    pallas_call x1, Pallas kernels: 36.6 us -> 36 us  [step_kernel(): pl.pallas_call(functools.partial(step_body, n), out_shape=[v((seqs, width...]
where the time goes in v5:
time: 37.5 us; the launch traced here: 37.3 us
  Pallas kernels  36.7 us (98%)
  between operations  0.65 us (2%)
    pallas_call x1, Pallas kernels, step_kernel(): pl.pallas_call(functools.partial(step_body, n), out_shape=[v((seqs, width...  36 us

profile of v5, /device:TPU:0, one launch (start us, length us, event | category | flops | bytes accessed | tf_op | source)
XLA Modules:
  0.0 37.3 jit_solution(11287646119315734131)
XLA Ops:
  0.6 36.0 %shard_map.201 = (bf16[16,2048]{1,0:T(8,128)(2,1)S(1)}, bf16[16,64]{1,0:T(8,128)(2,1)S(1)}, bf16[16,64]{1,0:T(8,128)(2,1)S(1)}, f32[16,16]{1,0:T(8,128)S(1)}) custom-call(s32[16]{0:T(128)} %len_hbm.1, f32[16]{0:T(128)} %fbias_hbm.1, bf16[16,2048]{1,0:T(8,128)(2,1)} %hid_hbm.1, bf16[2048]{0:T(1024)(128)(2,1)} %again_hbm.1, bf16[2048]{0:T(1024)(128)(2,1)} %fgain_hbm.1, ...), custom_call_target="tpu_custom_call" | custom-call | tf_op jit(solution)/shard_map/pallas_call | solution.py:629
  36.7 0.6 %shard_map.202 = (bf16[16,2048]{1,0:T(8,128)(2,1)}, bf16[16,64]{1,0:T(8,128)(2,1)}, bf16[16,64]{1,0:T(8,128)(2,1)}, f32[16,16]{1,0:T(8,128)}) custom-call(bf16[16,2048]{1,0:T(8,128)(2,1)S(1)} %get-tuple-element.12.refs_0_, bf16[16,64]{1,0:T(8,128)(2,1)S(1)} %get-tuple-element.13.refs_1_, bf16[16,64]{1,0:T(8,128)(2,1)S(1)} %get-tuple-element.14.refs_2_, ...), custom_call_target="tpu_custom_call" | custom-call | tf_op jit(solution)/shard_map/pallas_call | solution.py:663

commit v6 on v5

--- a/solution.py
+++ b/solution.py
@@ -151,7 +151,7 @@
               qw_hbm, kw_hbm, vw_hbm, fw_hbm, keys_hbm, vals_hbm, logs_hbm, ow_hbm, gate_hbm, up_hbm, down_hbm,
               out_ref, key_ref, val_ref, nlog_ref,
               len_ref, fbias_ref, hid_ref, again, fgain, fgain_row, ids_ref, rscore_ref, qw, kw, vw, fw, keys, vals, logs, scores, maxes, lasts, sums, mixed_heads, att, wsend, ow, gate, up, down,
-              hidl, part, mixl, mixin, rows, ssq, ssqp, scales, wts, begun, act, eout, back, fsum, far, upd,
+              hidl, part, mixl, mixin, rows, ssq, ssqp, scales, wts, act, eout, back, fsum, far, upd,
               send, recv, local):
     f32, bf16 = jnp.float32, jnp.bfloat16
     me, tp = lax.axis_index("ep"), lax.axis_index("tp")
@@ -166,6 +166,7 @@
     line = outer * seqs
     z, xy = me // PLANE, lax.rem(me, PLANE)
     x, y = lax.rem(xy, 2), xy // 2
+    kept = lax.rem(y + tp, 2)
     spots = [y * 2 + (1 - x), (1 - y) * 2 + x, (1 - y) * 2 + (1 - x)]
     plane = [z * PLANE + s for s in spots]
 
@@ -222,7 +223,8 @@
 
     barrier = pltpu.get_barrier_semaphore()
     for d in range(1, outer):
-        pl.semaphore_signal(barrier, inc=1, device_id=(zdev(lax.rem(z + d, outer)), tp), device_id_type=MESH)
+        for core in range(2):
+            pl.semaphore_signal(barrier, inc=1, device_id=(zdev(lax.rem(z + d, outer)), core), device_id_type=MESH)
     for p in plane:
         pl.semaphore_signal(barrier, inc=1, device_id=(p, tp), device_id_type=MESH)
     for p in plane[:2]:
@@ -230,7 +232,7 @@
     pl.semaphore_signal(barrier, inc=1, device_id=(me, 1 - tp), device_id_type=MESH)
 
     ow_load = load(ow_hbm.at[:, sl(tp, cols)], wsend)
-    first_core, slot, own_l = xy // 2, lax.rem(xy, 2), take("l")
+    slot, own_l = lax.rem(xy, 2), take("l")
 
     first = [load(hid_hbm, hid_ref), load(again_hbm, again), load(ids_hbm, ids_ref), load(rscore_hbm, rscore_ref)]
     scalars = [load(fbias_hbm, fbias_ref), load(len_hbm, len_ref), load(fgain_hbm, fgain)]
@@ -252,7 +254,7 @@
     def loaded(ref, l):
         pltpu.make_async_copy(ref, ref, local.at[l]).wait()
 
-    pl.semaphore_wait(barrier, outer - 1 + 3 + 2 + 1)
+    pl.semaphore_wait(barrier, 2 * (outer - 1) + 3 + 2 + 1)
 
     hf = feats // 2
     lo, hi = pl.ds(0, hf), pl.ds(hf, hf)
@@ -261,9 +263,9 @@
     quarters = [pl.ds(k * hf // 2, hf // 2) for k in range(4)]
     for i, some, r in ((0, quarters[0], 0), (1, quarters[2], 1), (0, quarters[1], 2), (1, quarters[3], 3),
                        (0, hi, 4), (1, lo, 4)):
-        begin(wsend.at[some], ow.at[slot, some, sl(tp, cols)], ow_s, ow_r + r, plane[i], first_core)
-
-    @pl.when(tp == first_core)
+        begin(wsend.at[some], ow.at[slot, some, sl(tp, cols)], ow_s, ow_r + r, plane[i], i)
+
+    @pl.when(tp == 0)
     def own_rows():
         load(ow_hbm, ow.at[slot], own_l)
 
@@ -287,9 +289,9 @@
     others = pl.ds(0, (outer - 1) * seqs)
     hid_s, hid_r = group(hidl.at[others]), take("r")
     for zz in zs:
-        begin(hid_ref.at[:, pl.ds(pl.multiple_of(zz * pf + tp * xq, xq), xq)], hidl.at[sl(z, seqs)],
+        begin(hid_ref.at[:, pl.ds(pl.multiple_of(zz * pf + kept * xq, xq), xq)], hidl.at[sl(z, seqs)],
               hid_s, hid_r, zdev(zz), tp)
-    hidl[sl(z, seqs), :] = hid_ref[:, pl.ds(pl.multiple_of(z * pf + tp * xq, xq), xq)]
+    hidl[sl(z, seqs), :] = hid_ref[:, pl.ds(pl.multiple_of(z * pf + kept * xq, xq), xq)]
     wt_s, wt_r = group(wts.at[0, others]), take("r")
     for zz in zs:
         begin(wts.at[3, sl(z, seqs)], wts.at[3, sl(z, seqs)], wt_s, wt_r, zdev(zz), tp)
@@ -389,19 +391,19 @@
         begin(att.at[tp, sl(z, seqs)], att.at[tp, sl(z, seqs)], att_s, att_r, zdev(zz), tp)
     relay_s, relay_r = group(ow.at[0, lo]), take("r")
 
-    @pl.when(tp == first_core)
+    @pl.when(tp == 0)
     def relay_along_y():
         for k in range(2):
             piece = ow.at[1 - slot, quarters[k]]
             arrived(piece, ow_r + 2 * k)
-            begin(piece, piece, relay_s, relay_r, plane[1], tp)
-
-    @pl.when(tp != first_core)
+            begin(piece, piece, relay_s, relay_r, plane[1], 1)
+
+    @pl.when(tp == 1)
     def relay_along_x():
         for k in range(2):
             piece = ow.at[slot, quarters[2 + k]]
             arrived(piece, ow_r + 1 + 2 * k)
-            begin(piece, piece, relay_s, relay_r, plane[0], tp)
+            begin(piece, piece, relay_s, relay_r, plane[0], 1)
 
     arrived(wts.at[0, others], wt_r)
     wline_s, wline_r = group(wts.at[pl.ds(0, 3)]), take("r")
@@ -413,7 +415,7 @@
     begin(att.at[tp], att.at[tp], both_s, both_r, me, 1 - tp)
     arrived(ow.at[0, lo], ow_r + 4)
 
-    @pl.when(tp == first_core)
+    @pl.when(tp == 0)
     def own_rows_there():
         loaded(ow.at[slot], own_l)
 
@@ -425,15 +427,15 @@
 
     project(slot)
 
-    @pl.when(tp != first_core)
+    @pl.when(tp == 1)
     def last_rows_there():
         arrived(ow.at[1 - slot], relay_r)
 
     project(1 - slot)
     mixed = jnp.concatenate([part[0], part[1]], axis=1).astype(bf16)
     residual = hidl[...].astype(f32) + mixed.astype(f32)
-    gain = fgain_row[:, pl.ds(pl.multiple_of(z * pf + tp * xq, xq), xq)]
-    block = tp * outer + z
+    gain = fgain_row[:, pl.ds(pl.multiple_of(z * pf + kept * xq, xq), xq)]
+    block = kept * outer + z
     rows[block, 3] = (residual * gain).astype(bf16)
     square = jnp.sum(residual * residual, axis=-1, keepdims=True)
     eye = (lax.broadcasted_iota(jnp.int32, (line, line), 0) == lax.broadcasted_iota(jnp.int32, (line, line), 1))
@@ -450,7 +452,7 @@
     mix_s, mix_r = group(mixl.at[others]), take("r")
 
     def out_to_plane(g, zz):
-        b, some = tp * outer + zz, rows_of(g, z)
+        b, some = kept * outer + zz, rows_of(g, z)
         for i in (2, 0, 1):
             begin(rows.at[b, 3, some], rows.at[b, i, some], prow_s, prow_r + g, plane[i], tp)
 
@@ -462,51 +464,49 @@
             for zz in reversed(zs):
                 begin(ssq.at[z, 3], ssq.at[z, 3], zsq_s, zsq_r, zdev(zz), tp)
         out_to_plane(g, z)
-    mixin[z] = mixl[sl(z, seqs), :]
+    swap_s, swap_r = take("s"), take("r")
+
+    @pl.when(y == 0)
+    def mixed_stays():
+        mixin[z] = mixl[sl(z, seqs), :]
+
+    @pl.when(y == 1)
+    def mixed_swaps():
+        begin(mixl.at[sl(z, seqs)], mixin.at[z], 4, swap_r, me, 1 - tp)
+
     for g in range(outer):
         if g:
             arrived(rows.at[pl.ds(0, outer - 1), 3, rows_of(g, z)], zrow_r + outer - 1 + g)
         for zz in zs:
             if g == 0:
-                arrived(rows.at[tp * outer + zz, 3, rows_of(g, z)], zrow_r + zz)
+                arrived(rows.at[kept * outer + zz, 3, rows_of(g, z)], zrow_r + zz)
             out_to_plane(g, zz)
         if g == 0:
             arrived(ssq.at[0, pl.ds(0, outer - 1)], zsq_r)
             for i in range(3):
                 begin(ssq.at[:, 3], ssq.at[:, i], psq_s, psq_r, plane[i], tp)
     for zz in zs:
-        begin(mixl.at[sl(zz, seqs)], mixin.at[z], mix_s, mix_r, zdev(zz), tp)
+        begin(mixl.at[sl(zz, seqs)], mixin.at[z], mix_s, mix_r, zdev(zz), kept)
     units = gate.shape[2]
     loaded(qw.at[pl.ds(0, (2 * width * units + units * width // 2) // cols)], expert_l)
     arrived(wts.at[pl.ds(0, 3)], wline_r)
 
     parts = [[g] for g in range(outer)]
 
-    def product(part_groups, t):
-        left = jnp.concatenate([
-            jnp.concatenate([rows[t * outer + i, :, rows_of(g, z), :].reshape(PLANE * seqs, xq) for g in part_groups],
-                            axis=0) for i in range(outer)], axis=1)
-        span = pl.ds(t * outer, outer)
-        return [jnp.dot(left, w[span].reshape(outer * xq, w.shape[2]), preferred_element_type=f32) for w in (gate, up)]
-
     def pass_on(part_groups):
         for g in part_groups:
-            span, some = pl.ds(tp * outer, outer), rows_of(g, z)
-            arrived(rows.at[span, pl.ds(0, 3), some], prow_r + g)
-            block_rows = rows.at[span, :, some]
-            begin(block_rows, block_rows, crow_s, crow_r + g, me, 1 - tp)
-
-    def start(part_groups):
-        k = part_groups[0] % 2
-        for i, v in enumerate(product(part_groups, tp)):
-            begun[k, i] = v
-        return k
-
-    def collect(part_groups, k):
+            mine, theirs, some = pl.ds(kept * outer, outer), pl.ds((1 - kept) * outer, outer), rows_of(g, z)
+            arrived(rows.at[pl.ds(0, outer), pl.ds(0, 3), some], prow_r + g)
+            for ref in (rows.at[theirs, pl.ds(1, 2), some], rows.at[mine, 0, some], rows.at[mine, 3, some]):
+                begin(ref, ref, crow_s, crow_r + g, me, 1 - tp)
+
+    def collect(part_groups):
         for g in part_groups:
-            arrived(rows.at[pl.ds((1 - tp) * outer, outer), :, rows_of(g, z)], crow_r + g)
-        late = product(part_groups, 1 - tp)
-        return begun[k, 0] + late[0], begun[k, 1] + late[1]
+            arrived(rows.at[pl.ds(0, outer), :, rows_of(g, z)], crow_r + g)
+        left = jnp.concatenate([
+            jnp.concatenate([rows[b, :, rows_of(g, z), :].reshape(PLANE * seqs, xq) for g in part_groups], axis=0)
+            for b in range(2 * outer)], axis=1)
+        return [jnp.dot(left, w[...].reshape(width, w.shape[2]), preferred_element_type=f32) for w in (gate, up)]
 
     act_s, act_r = group(act.at[0]), take("r", outer)
 
@@ -547,9 +547,8 @@
         squares = squares + ssq[i]
     ssqp[tp] = squares
     begin(ssqp.at[tp], ssqp.at[tp], csq_s, csq_r, me, 1 - tp)
-    early = start(parts[0])
     pass_on(parts[1])
-    a, u = collect(parts[0], early)
+    a, u = collect(parts[0])
     arrived(ssqp.at[1 - tp], csq_r)
     squares = ssqp[0] + ssqp[1]
     for q in range(PLANE):
@@ -573,12 +572,11 @@
 
     last = len(parts) - 1
     for k in range(1, len(parts)):
-        early = start(parts[k])
         if k == last:
             give(parts[k - 1])
         elif k > 1:
             pass_on(parts[k + 1])
-        a, u = collect(parts[k], early)
+        a, u = collect(parts[k])
         activate(parts[k], a, u)
         if k == 1:
             pass_on(parts[2])
@@ -589,6 +587,12 @@
     for g in range(1, outer):
         summed = near(g)
     arrived(mixin.at[pl.ds(0, outer - 1)], mix_r)
+
+    @pl.when(y == 1)
+    def mixed_swapped():
+        arrived(mixin.at[z], swap_r)
+        copy(mixl.at[sl(z, seqs)], mixin.at[z], 4, 0, me, 1 - tp).wait_send()
+
     arrived(far.at[pl.ds(0, outer - 1)], far_r)
     for zz in zs:
         summed = summed + far[zz].astype(f32)
@@ -644,10 +648,10 @@
             v((outer, seqs, xq), bf16),
             v((2 * outer, PLANE, line, xq), bf16), v((outer, PLANE, 8, line), f32), v((2, PLANE, 8, line), f32),
             v((PLANE, line, 128), f32), v((PLANE, line, 128), f32),
-                        v((2, 2, PLANE * seqs, units), f32), v((2, outer, PLANE * seqs, units), bf16),
+                        v((2, outer, PLANE * seqs, units), bf16),
             v((outer, PLANE, seqs, half), bf16), v((outer, 3, seqs, half), bf16),
             v((outer, seqs, half), bf16), v((outer, seqs, half), bf16), v((2, seqs, half), bf16),
-            pltpu.SemaphoreType.DMA((4,)), pltpu.SemaphoreType.DMA((17 + 6 * outer,)), pltpu.SemaphoreType.DMA((15,)),
+            pltpu.SemaphoreType.DMA((5,)), pltpu.SemaphoreType.DMA((18 + 6 * outer,)), pltpu.SemaphoreType.DMA((15,)),
         ],
         compiler_params=pltpu.CompilerParams(
             collective_id=0, has_side_effects=True, vmem_limit_bytes=40 * 1024 * 1024),

time: 37.5 us -> 37.3 us (level)
  no operation moved by 1% of the time
where the time goes in v6:
time: 37.3 us; the launch traced here: 37.1 us
  Pallas kernels  36.5 us (98%)
  between operations  0.65 us (2%)
    pallas_call x1, Pallas kernels, step_kernel(): pl.pallas_call(functools.partial(step_body, n), out_shape=[v((seqs, width...  35.9 us

profile of v6, /device:TPU:0, one launch (start us, length us, event | category | flops | bytes accessed | tf_op | source)
XLA Modules:
  0.0 37.1 jit_solution(9678694664755087334)
XLA Ops:
  0.6 35.9 %shard_map.201 = (bf16[16,2048]{1,0:T(8,128)(2,1)S(1)}, bf16[16,64]{1,0:T(8,128)(2,1)S(1)}, bf16[16,64]{1,0:T(8,128)(2,1)S(1)}, f32[16,16]{1,0:T(8,128)S(1)}) custom-call(s32[16]{0:T(128)} %len_hbm.1, f32[16]{0:T(128)} %fbias_hbm.1, bf16[16,2048]{1,0:T(8,128)(2,1)} %hid_hbm.1, bf16[2048]{0:T(1024)(128)(2,1)} %again_hbm.1, bf16[2048]{0:T(1024)(128)(2,1)} %fgain_hbm.1, ...), custom_call_target="tpu_custom_call" | custom-call | tf_op jit(solution)/shard_map/pallas_call | solution.py:633
  36.5 0.6 %shard_map.202 = (bf16[16,2048]{1,0:T(8,128)(2,1)}, bf16[16,64]{1,0:T(8,128)(2,1)}, bf16[16,64]{1,0:T(8,128)(2,1)}, f32[16,16]{1,0:T(8,128)}) custom-call(bf16[16,2048]{1,0:T(8,128)(2,1)S(1)} %get-tuple-element.12.refs_0_, bf16[16,64]{1,0:T(8,128)(2,1)S(1)} %get-tuple-element.13.refs_1_, bf16[16,64]{1,0:T(8,128)(2,1)S(1)} %get-tuple-element.14.refs_2_, ...), custom_call_target="tpu_custom_call" | custom-call | tf_op jit(solution)/shard_map/pallas_call | solution.py:667
